TPU v7x, 512 devices: a whole 4x4x16 slice. The times are simulated.
512 devices in a mesh: sp: 32 (over z, core), tp: 16 (over y, x).
Axes of the slice: x: 4, y: 4, z: 16, core: 2. Of those that a mesh axis runs over, the one named last changes fastest.
Arguments:
- cotangent: bfloat16 [4096, 2048], P('sp'), may hold values from -6 to 6
- stream: bfloat16 [4096, 2048], P('sp'), may hold values from -6 to 6
- routes: int32 [4096, 2], P('sp'), may hold values from 0 to 15, all different within a row; in each aligned block of 128 rows (0 to 127, 128 to 255, ...) at most 20 rows name the same one
- route_weights: float32 [4096, 2], P('sp'), may hold values from 0.2 to 1
- gate_proj: bfloat16 [32, 2048, 2048], P('sp', None, 'tp'), may hold values from -0.125 to 0.125
- up_proj: bfloat16 [32, 2048, 2048], P('sp', None, 'tp'), may hold values from -0.125 to 0.125
- down_proj: bfloat16 [32, 2048, 2048], P('sp', 'tp'), may hold values from -0.09375 to 0.09375
- out_weight: bfloat16 [2048, 8192], P('sp', 'tp'), may hold values from -0.0625 to 0.0625
- queries: bfloat16 [4096, 4096], P('sp', 'tp'), may hold values from -6 to 6
- keys: bfloat16 [4096, 4096], P('sp', 'tp'), may hold values from -6 to 6
- values: bfloat16 [4096, 8192], P('sp', 'tp'), may hold values from -6 to 6
- decay_rate: float32 [16], P('tp'), may hold values from 0 to 1
Outputs:
- grad_gate: bfloat16 [32, 2048, 2048], P('sp', None, 'tp')
- grad_up: bfloat16 [32, 2048, 2048], P('sp', None, 'tp')
- grad_down: bfloat16 [32, 2048, 2048], P('sp', 'tp')
- grad_out_weight: float32 [2048, 8192], P('sp', 'tp')
- grad_queries: bfloat16 [4096, 4096], P('sp', 'tp')
- grad_keys: bfloat16 [4096, 4096], P('sp', 'tp')
- grad_values: bfloat16 [4096, 8192], P('sp', 'tp')
Inputs may be any that keep to these rules, and one draw needn't show every extreme that they name: `routes`: each row names two different experts. In each block of 128 consecutive tokens no expert is named more than 20 times, and in some block of every draw one expert is named exactly 20 times.
All inputs are finite; a program needn't handle non-finite values.
Results may differ from a plain program's by a relative error of at most 0.006.
Values may be sent and summed in bfloat16 or wider, within the bound.
A program may use at most 128 MiB of HBM per device.

v0:
```python
import jax
import jax.numpy as jnp
from jax import lax
from jax.sharding import Mesh
from jax.sharding import PartitionSpec as P

SP = ("sp_0", "sp_1")


NORM_EPS = 1.0
precise_setting = lax.Precision.HIGHEST


def nothing_yet(array, identity):
    return jax.tree.map(
        lambda part, zero: jnp.zeros_like(part) + jnp.asarray(zero, part.dtype), array, identity
    )


def entering(array, axes, combine, identity):
    before = start = nothing_yet(array, identity)
    running = array
    for axis in reversed(axes):
        length, index = (lax.axis_size(axis), lax.axis_index(axis))
        pieces = jax.tree.map(lambda part: lax.all_gather(part, axis), running)
        inside, running = (start, start)
        for k in range(length):
            passed = k < index
            running = combine(running, jax.tree.map(lambda part: part[k], pieces))
            inside = jax.tree.map(lambda new, old: jnp.where(passed, new, old), running, inside)
        before = combine(inside, before)
    return before


def swapped(block, axis, apart):
    count = lax.axis_size(axis)
    route = []
    for low in range(count):
        high = low | 1 << apart
        if high != low and high < count:
            route += [(low, high), (high, low)]
    return lax.ppermute(block, axis, route)


def reduced_to_own(pieces, axes, sequence):
    lengths = [lax.axis_size(a) for a in axes]
    pieces = pieces.reshape(*lengths, *pieces.shape[1:])
    pieces = pieces.transpose(*sequence, *range(len(axes), pieces.ndim))
    pieces = pieces.reshape(-1, *pieces.shape[len(axes) :])
    for k in sequence:
        pieces = lax.psum_scatter(pieces, axes[k], scatter_dimension=0, tiled=True)
    return pieces[0]


def split_up(array, dim, length):
    before, after = (array.shape[:dim], array.shape[dim + 1 :])
    return jnp.moveaxis(array.reshape(*before, length, -1, *after), dim, 0)


def sum_by_axis(array, axes, sequence, dim):
    length = lax.axis_size(axes)
    return reduced_to_own(split_up(array, dim, length), axes, sequence)


def joined_along(pieces, dim):
    pieces = jnp.moveaxis(pieces, 0, dim)
    lengths = pieces.shape
    return pieces.reshape(*lengths[:dim], lengths[dim] * lengths[dim + 1], *lengths[dim + 2 :])


def gather_in_order(array, axes, sequence):
    pieces = array[None]
    for k in sequence:
        pieces = lax.all_gather(pieces, axes[k], axis=0, tiled=True)
    carried = [lax.axis_size(axes[k]) for k in reversed(sequence)]
    pieces = pieces.reshape(*carried, *array.shape)
    turned = sorted(range(len(sequence)), key=lambda place: sequence[len(sequence) - 1 - place])
    return pieces.transpose(*turned, *range(len(sequence), pieces.ndim)).reshape(-1, *array.shape)


def gather_axes(array, axes, sequence, dim):
    return joined_along(gather_in_order(array, axes, sequence), dim)


def entering_2(part, axis, combine, identity):
    count = lax.axis_size(axis)
    place = lax.axis_index(axis)
    ahead = count - 1 - place
    gathered = jax.tree.map(lambda a: lax.all_gather(a, axis), part)
    state = jax.tree.map(lambda a, e: jnp.zeros_like(a) + jnp.asarray(e, a.dtype), part, identity)

    def one(hop, state):
        source = count - 1 - hop
        return combine(
            state, jax.tree.map(lambda a: lax.dynamic_index_in_dim(a, source, 0, False), gathered)
        )

    return lax.fori_loop(0, ahead, one, state)


def silu_grad(pre_act):
    sigmoid = jax.nn.sigmoid(pre_act)
    return sigmoid * (1.0 + pre_act * (1.0 - sigmoid))


def chain_join(earlier, latter):
    return (earlier[0] * latter[0], latter[0] * earlier[1] + latter[1])


def local(
    cotangent,
    stream,
    routes,
    route_weights,
    gate_proj,
    up_proj,
    down_proj,
    out_weight,
    queries,
    keys,
    values,
    decay_rate,
):
    tok_rows, model_width = cotangent.shape
    top_count = routes.shape[1]
    seq_devices = lax.axis_size(SP)
    tp_devices = lax.axis_size("tp")
    experts = seq_devices // 2
    slot_count = 5 * tok_rows // seq_devices
    assigned = tok_rows * top_count
    buffer_rows = seq_devices * slot_count
    col_width = model_width // tp_devices
    heads_here = decay_rate.shape[0]
    key_dim = queries.shape[1] // heads_here
    value_dim = values.shape[1] // heads_here
    query_wide_float = (
        queries.astype(jnp.float32).reshape(tok_rows, heads_here, key_dim).transpose(1, 0, 2)
    )
    key_wide_float = keys.astype(jnp.float32).reshape(tok_rows, heads_here, key_dim).transpose(
        1, 0, 2
    ) * key_dim ** (-0.5)
    value_wide_float = (
        values.astype(jnp.float32).reshape(tok_rows, heads_here, value_dim).transpose(1, 0, 2)
    )
    local_steps = jnp.arange(tok_rows, dtype=jnp.float32)
    distance = local_steps[:, None] - local_steps[None, :]
    decay_mask_matrix = jnp.where(
        distance >= 0, jnp.exp(-decay_rate[:, None, None] * jnp.maximum(distance, 0.0)), 0.0
    )
    enter_decay = jnp.exp(-decay_rate[:, None] * (local_steps + 1.0))[:, :, None]
    leave_decay = jnp.exp(-decay_rate[:, None] * (tok_rows - 1.0 - local_steps))[:, :, None]
    start_decay = jnp.exp(-decay_rate[:, None] * local_steps)[:, :, None]
    trailing_decay = jnp.exp(-decay_rate[:, None] * (tok_rows - local_steps))[:, :, None]
    block_decay = jnp.exp(-decay_rate * tok_rows)[:, None, None]
    identity = (
        jnp.ones((heads_here, 1, 1), jnp.float32),
        jnp.zeros((heads_here, key_dim, value_dim), jnp.float32),
    )
    local_state = jnp.einsum(
        "hld,hle->hde", key_wide_float * leave_decay, value_wide_float, precision=precise_setting
    )
    _, carried = entering((block_decay, local_state), SP, chain_join, identity)
    expert_ids = routes.reshape(assigned)
    onehot = (expert_ids[:, None] == jnp.arange(experts, dtype=jnp.int32)[None, :]).astype(
        jnp.int32
    )
    slot_rank = jnp.sum((jnp.cumsum(onehot, axis=0) - 1) * onehot, axis=1)
    target = expert_ids * slot_count + slot_rank
    slot_index = jnp.arange(experts * slot_count, dtype=jnp.int32)[:, None]
    place_pairs = (slot_index == target[None, :]).astype(jnp.bfloat16)
    target_pairs = target.reshape(tok_rows, top_count)
    place_tokens = jnp.zeros((experts * slot_count, tok_rows), jnp.float32)
    for choice_index in range(top_count):
        place_tokens = place_tokens + (slot_index == target_pairs[:, choice_index][None, :]).astype(
            jnp.float32
        )
    scaled = (
        (route_weights[:, :, None] * cotangent[:, None, :].astype(jnp.float32))
        .reshape(assigned, model_width)
        .astype(jnp.bfloat16)
    )
    cot_send = jnp.dot(place_pairs, scaled, preferred_element_type=jnp.float32).astype(jnp.bfloat16)
    row_send = jnp.dot(
        place_tokens.astype(jnp.bfloat16), stream, preferred_element_type=jnp.float32
    ).astype(jnp.bfloat16)
    packed = jnp.stack([cot_send, row_send]).reshape(2, experts, slot_count, model_width)
    half_slots = slot_count // 2
    own_half = lax.all_to_all(
        packed.reshape(2, seq_devices, half_slots, model_width),
        SP,
        split_axis=1,
        concat_axis=1,
        tiled=True,
    )
    partner_half = swapped(own_half, SP, 0)
    is_lower = lax.axis_index(SP) % 2 == 0
    received = jnp.where(
        is_lower,
        jnp.concatenate([own_half, partner_half], axis=2),
        jnp.concatenate([partner_half, own_half], axis=2),
    )
    received = received.reshape(2, buffer_rows, model_width)
    cot_rows = received[0]
    in_rows = received[1]
    gate_here = gate_proj[0]
    up_here = up_proj[0]
    down_here = down_proj[0]
    along_cols = (((1,), (1,)), ((), ()))
    along_rows = (((0,), (0,)), ((), ()))
    pre_gate = jnp.dot(in_rows, gate_here, preferred_element_type=jnp.float32)
    pre_up = jnp.dot(in_rows, up_here, preferred_element_type=jnp.float32)
    active = jax.nn.silu(pre_gate)
    hidden = (active * pre_up).astype(jnp.bfloat16)
    grad_hidden = lax.dot_general(
        cot_rows, down_here, along_cols, preferred_element_type=jnp.float32
    )
    grad_pre_gate = (grad_hidden * pre_up * silu_grad(pre_gate)).astype(jnp.bfloat16)
    grad_pre_up = (grad_hidden * active).astype(jnp.bfloat16)
    joined_grads = jnp.concatenate([grad_pre_gate, grad_pre_up], axis=1)
    joined_weights = jnp.concatenate([gate_here, up_here], axis=1)
    partial_in = lax.dot_general(
        joined_grads, joined_weights, along_cols, preferred_element_type=jnp.float32
    ).astype(jnp.bfloat16)
    pieces = lax.all_to_all(partial_in, "tp", split_axis=1, concat_axis=0, tiled=True)
    grad_gate = lax.dot_general(
        in_rows, grad_pre_gate, along_rows, preferred_element_type=jnp.float32
    ).astype(jnp.bfloat16)
    grad_up = lax.dot_general(
        in_rows, grad_pre_up, along_rows, preferred_element_type=jnp.float32
    ).astype(jnp.bfloat16)
    grad_down = lax.dot_general(
        hidden, cot_rows, along_rows, preferred_element_type=jnp.float32
    ).astype(jnp.bfloat16)
    summed = jnp.sum(pieces.reshape(tp_devices, buffer_rows, col_width).astype(jnp.float32), axis=0)
    returned = lax.all_to_all(
        summed.reshape(seq_devices, slot_count, col_width),
        SP,
        split_axis=0,
        concat_axis=0,
        tiled=True,
    )
    per_slot = jnp.sum(returned.reshape(experts, 2, slot_count, col_width), axis=1).reshape(
        experts * slot_count, col_width
    )
    token_grad = lax.dot_general(
        place_tokens,
        per_slot,
        along_rows,
        precision=precise_setting,
        preferred_element_type=jnp.float32,
    )
    own_cols = lax.dynamic_slice_in_dim(cotangent, lax.axis_index("tp") * col_width, col_width, 1)
    mid_cols = (own_cols.astype(jnp.float32) + token_grad).astype(jnp.bfloat16)
    mid_grad = lax.all_gather(mid_cols, "tp", axis=1, tiled=True)
    attention_scores = (
        jnp.einsum("niv,nov->nio", query_wide_float, key_wide_float, precision=precise_setting)
        * decay_mask_matrix
    )
    retained = jnp.einsum(
        "hlm,hme->hle", attention_scores, value_wide_float, precision=precise_setting
    )
    retained = retained + enter_decay * jnp.einsum(
        "hld,hde->hle", query_wide_float, carried, precision=precise_setting
    )
    centered = retained - jnp.mean(retained, axis=-1, keepdims=True)
    inv_scale = lax.rsqrt(jnp.mean(centered * centered, axis=-1, keepdims=True) + NORM_EPS)
    normed = centered * inv_scale
    mixed = normed.transpose(1, 0, 2).reshape(tok_rows, heads_here * value_dim).astype(jnp.bfloat16)
    row_block = mid_grad
    grad_out_weight = sum_by_axis(
        lax.dot_general(row_block, mixed, along_rows, preferred_element_type=jnp.float32),
        SP,
        (1, 0),
        0,
    )
    row_block = mid_grad
    grad_mixed = jnp.dot(
        row_block, gather_axes(out_weight, SP, (0, 1), 0), preferred_element_type=jnp.float32
    )
    head_grad = grad_mixed.reshape(tok_rows, heads_here, value_dim).transpose(1, 0, 2)
    grad_retained = inv_scale * (
        head_grad
        - jnp.mean(head_grad, axis=-1, keepdims=True)
        - normed * jnp.mean(head_grad * normed, axis=-1, keepdims=True)
    )
    score_gradient = (
        jnp.einsum("hle,hme->hlm", grad_retained, value_wide_float, precision=precise_setting)
        * decay_mask_matrix
    )
    query_gradient = jnp.einsum(
        "nzs,nst->nzt", score_gradient, key_wide_float, precision=precise_setting
    )
    query_gradient = query_gradient + enter_decay * jnp.einsum(
        "hle,hde->hld", grad_retained, carried, precision=precise_setting
    )
    local_back = jnp.einsum(
        "hld,hle->hde", query_wide_float * start_decay, grad_retained, precision=precise_setting
    )
    _, incoming_future_state = entering_2((block_decay, local_back), SP, chain_join, identity)
    key_gradient = jnp.einsum(
        "nkp,nkg->npg", score_gradient, query_wide_float, precision=precise_setting
    )
    key_gradient = (
        key_gradient
        + trailing_decay
        * jnp.einsum(
            "pgt,pyt->pgy", value_wide_float, incoming_future_state, precision=precise_setting
        )
    ) * key_dim ** (-0.5)
    grad_v = jnp.einsum("hlm,hle->hme", attention_scores, grad_retained, precision=precise_setting)
    grad_v = grad_v + trailing_decay * jnp.einsum(
        "bix,bxo->bio", key_wide_float, incoming_future_state, precision=precise_setting
    )
    grad_queries = (
        query_gradient.transpose(1, 0, 2)
        .reshape(tok_rows, heads_here * key_dim)
        .astype(jnp.bfloat16)
    )
    grad_keys = (
        key_gradient.transpose(1, 0, 2).reshape(tok_rows, heads_here * key_dim).astype(jnp.bfloat16)
    )
    grad_values = (
        grad_v.transpose(1, 0, 2).reshape(tok_rows, heads_here * value_dim).astype(jnp.bfloat16)
    )
    return (
        grad_gate[None],
        grad_up[None],
        grad_down[None],
        grad_out_weight,
        grad_queries,
        grad_keys,
        grad_values,
    )


def solution(mesh):
    split = Mesh(mesh.devices.reshape(16, 2, mesh.shape["tp"]), ("sp_0", "sp_1", "tp"))
    in_specs = (
        P(SP, None),
        P(SP, None),
        P(SP, None),
        P(SP, None),
        P(SP, None, "tp"),
        P(SP, None, "tp"),
        P(SP, "tp", None),
        P(SP, "tp"),
        P(SP, "tp"),
        P(SP, "tp"),
        P(SP, "tp"),
        P("tp"),
    )
    out_specs = (
        P(SP, None, "tp"),
        P(SP, None, "tp"),
        P(SP, "tp", None),
        P(SP, "tp"),
        P(SP, "tp"),
        P(SP, "tp"),
        P(SP, "tp"),
    )
    return jax.shard_map(local, mesh=split, in_specs=in_specs, out_specs=out_specs, check_vma=False)
```

profile of v0, /device:TPU:1, one launch (start us, length us, event | category | flops | bytes accessed | tf_op | source)
XLA Modules:
  0.0 609.8 jit_solution(42253591637407201)
XLA Ops:
  13.3 2.5 mul.571
  16.0 3.4 convolution_convert_fusion.2
  19.4 3.3 stack.9
  22.8 2.1 pad_maximum_fusion
  24.9 4.3 copy.72
  29.2 16.9 %all-to-all-start = ((bf16[2,32,10,2048]{3,0,2,1:T(2,128)(2,1)}), bf16[2,32,10,2048]{3,0,2,1:T(2,128)(2,1)S(1)}, u32[]{:S(2)}, u32[]{:S(2)}) async-start(bf16[2,32,10,2048]{3,0,2,1:T(2,128)(2,1)} %copy.72), calls=%async_computation | async-start | bytes 5242880 | tf_op jit(solution)/shard_map/all_to_all | solution.py:188
  50.9 2.5 all-reduce
  54.6 16.6 %all-gather.16.cloned.1.call-done = f32[512,512]{1,0:T(8,128)} async-done(((f32[256,512]{1,0:T(8,128)}), f32[512,512]{1,0:T(8,128)}) %all-gather.16.cloned.1.call-update) | async-done | bytes 1048592 | tf_op jit(solution)/shard_map/all_gather | solution.py:25
  71.3 2.7 fusion.23
  74.0 102.0 %all-to-all-done = bf16[2,32,10,2048]{3,0,2,1:T(2,128)(2,1)S(1)} async-done(((bf16[2,32,10,2048]{3,0,2,1:T(2,128)(2,1)}), bf16[2,32,10,2048]{3,0,2,1:T(2,128)(2,1)S(1)}, u32[]{:S(2)}, u32[]{:S(2)}) %all-to-all-start) | async-done | bytes 2621472 | tf_op jit(solution)/shard_map/all_to_all | solution.py:188
  176.0 3.0 copy.73
  179.0 3.3 collective-permute-start
  182.3 4.7 collective-permute-done
  186.9 4.4 copy.74
  191.4 24.8 %broadcast_select_fusion = bf16[2,32,20,2048]{3,0,2,1:T(2,128)(2,1)} fusion(pred[]{:T(512)S(6)} %eq.71, bf16[2,32,10,2048]{3,0,2,1:T(2,128)(2,1)S(1)} %copy.74, bf16[2,32,10,2048]{3,0,2,1:T(2,128)(2,1)S(1)} %all-to-all-done), kind=kLoop, calls=%fused_computation.2 | loop fusion | flops 7864320 | bytes 10485761 | tf_op jit(solution)/shard_map/jit(_where)/select_n | solution.py:197
  216.1 27.2 %slice_reduce_fusion = (bf16[32,20,2048]{2,1,0:T(8,128)(2,1)}, bf16[32,20,2048]{2,1,0:T(8,128)(2,1)}) fusion(bf16[2,32,20,2048]{3,0,2,1:T(2,128)(2,1)} %broadcast_select_fusion), kind=kLoop, calls=%fused_computation.3 | loop fusion | bytes 10485760 | tf_op jit(solution)/shard_map/slice | solution.py:203
  243.4 3.7 squeeze.25
  247.0 5.2 squeeze.26
  252.3 2.1 fusion.62
  258.7 40.2 %all_to_all.23 = bf16[640,16,128]{2,0,1:T(8,128)(2,1)S(1)} all-to-all(bf16[640,16,128]{2,0,1:T(8,128)(2,1)S(1)} %bitcast.161), channel_id=1, replica_groups=mesh['sp_0'=16,'sp_1'=2,'tp'=16] {'tp'}, dimensions={1} | all-to-all | bytes 5242880 | tf_op jit(solution)/shard_map/all_to_all | solution.py:224
  300.0 6.8 %all-to-all-start.2 = ((f32[32,20,128]{2,1,0:T(8,128)}), f32[32,20,128]{2,1,0:T(8,128)S(1)}, u32[]{:S(2)}, u32[]{:S(2)}) async-start(f32[32,20,128]{2,1,0:T(8,128)} %reshape.473), calls=%async_computation.2 | async-start | bytes 786432 | tf_op jit(solution)/shard_map/all_to_all | solution.py:235
  310.2 34.0 %all-reduce.1 = f32[16]{0:T(128)S(1)} all-reduce(f32[16]{0:T(128)S(1)} %bitcast_dynamic-update-slice_fusion), channel_id=3, replica_groups=mesh['sp_0'=16,'sp_1'=2,'tp'=16] {'sp_0'}, use_global_device_ids=true, to_apply=%add.1 | all-reduce | flops 16 | bytes 128
  350.4 16.9 %all_gather.37 = bf16[128,2048]{1,0:T(8,128)(2,1)S(1)} all-gather(bf16[128,128]{1,0:T(8,128)(2,1)S(1)} %fusion.14), channel_id=1, replica_groups=mesh['sp_0'=16,'sp_1'=2,'tp'=16] {'tp'}, dimensions={1}, use_global_device_ids=true | all-gather | bytes 557056 | tf_op jit(solution)/shard_map/all_gather | solution.py:254
  368.4 14.7 %fusion.22 = f32[256,512]{1,0:T(8,128)S(1)} fusion(f32[16,1,256,512]{3,2,1,0:T(8,128)} %all-gather.12.cloned.1.call-done, f32[512,512]{1,0:T(8,128)} %all-gather.16.cloned.1.call-done, f32[]{:T(128)} %bitcast.41, f32[]{:T(128)} %bitcast.39, f32[]{:T(128)} %bitcast.38, f32[]{:T(128)} %bitcast.37, f32[]{:T(128)} %bitcast.36, f32[]{:T(128)} %bitcast.35, ...), kind=kLoop, calls=%fused_computation.47 | loop fusion | flops 7077888 | bytes 9961566 | tf_op jit(solution)/shard_map/add | solution.py:107
  384.6 2.5 copy.79
  387.3 1.8 copy.80
  392.5 26.6 %reduce-scatter.3.cloned.1.call-done = f32[16,64,512]{2,1,0:T(8,128)} async-done(((f32[32,64,512]{2,1,0:T(8,128)}), f32[16,64,512]{2,1,0:T(8,128)}) %reduce-scatter.3.cloned.1.call-update) | async-done | bytes 2097168 | tf_op jit(solution)/shard_map/reduce_scatter | solution.py:51
  421.1 48.9 %all-reduce.2 = f32[32]{0:T(128)S(1)} all-reduce(f32[32]{0:T(128)S(1)} %fusion.60), channel_id=6, replica_groups=mesh['sp_0'=16,'sp_1'=2,'tp'=16] {'sp_0','sp_1'}, use_global_device_ids=true, to_apply=%add.2 | all-reduce | flops 32 | bytes 256
  470.1 2.7 fusion
  478.3 50.8 %all-gather.20.cloned.1.call-done = f32[8192,512]{1,0:T(8,128)} async-done(((f32[256,512]{1,0:T(8,128)}), f32[8192,512]{1,0:T(8,128)}) %all-gather.20.cloned.1.call-update) | async-done | bytes 16777232 | tf_op jit(solution)/shard_map/all_gather | solution.py:89
  529.2 71.2 %while.14 = (s32[]{:T(128)}, f32[1,256,512]{2,1,0:T(8,128)S(1)}, s32[]{:T(128)}, f32[32,1,1,1]{0,3,2,1:T(1,128)S(1)}, f32[32,1,256,512]{3,2,1,0:T(8,128)}, /*index=5*/s32[]{:T(128)}, s32[]{:T(128)}, s32[]{:T(128)}, s32[]{:T(128)}) while((s32[]{:T(128)}, f32[1,256,512]{2,1,0:T(8,128)S(1)}, s32[]{:T(128)}, f32[32,1,1,1]{0,3,2,1:T(1,128)S(1)}, ...), condition=%wide.region_12.13_spmd, body=%wide.region_11.12_spmd.sunk | while | flops 262150 | bytes 1573031 | solution.py:98
  546.4 1.8 bitcast_add_fusion.2
  551.1 1.8 bitcast_add_fusion.2
  553.5 1.8 bitcast_add_fusion.2
  555.8 1.8 bitcast_add_fusion.2
  558.2 1.8 bitcast_add_fusion.2
  560.6 1.8 bitcast_add_fusion.2
  563.0 1.8 bitcast_add_fusion.2
  565.3 1.8 bitcast_add_fusion.2
  570.1 1.8 bitcast_add_fusion.2
  572.5 1.8 bitcast_add_fusion.2
  574.8 1.8 bitcast_add_fusion.2
  577.2 1.8 bitcast_add_fusion.2
  579.6 1.8 bitcast_add_fusion.2
  581.9 1.8 bitcast_add_fusion.2
  584.3 1.8 bitcast_add_fusion.2
  589.1 1.8 bitcast_add_fusion.2
  591.4 1.8 bitcast_add_fusion.2
  (188 shorter events, 79.4 us)
Async XLA Ops:
  7.2 3.0 copy-start
  10.2 2.1 copy-start.14
  13.3 2.5 copy-start.28
  16.0 6.7 %copy-start.4 = (bf16[1,32,10,2048]{3,2,1,0:T(8,128)(2,1)S(1)}, bf16[1,32,10,2048]{3,2,1,0:T(8,128)(2,1)}, u32[]{:S(2)}) copy-start(bf16[1,32,10,2048]{3,2,1,0:T(8,128)(2,1)} %stack.10) | copy-start | bytes 3932164
  29.2 17.6 %copy-start.8 = (bf16[128,512]{1,0:T(8,128)(2,1)S(1)}, bf16[128,512]{1,0:T(8,128)(2,1)}, u32[]{:S(2)}) copy-start(bf16[128,512]{1,0:T(8,128)(2,1)} %param.24) | copy-start | bytes 393220
  29.2 17.6 %copy-start.19 = (bf16[128,256]{1,0:T(8,128)(2,1)S(1)}, bf16[128,256]{1,0:T(8,128)(2,1)}, u32[]{:S(2)}) copy-start(bf16[128,256]{1,0:T(8,128)(2,1)} %param.23) | copy-start | bytes 196612
  29.2 146.8 %all-to-all-start = ((bf16[2,32,10,2048]{3,0,2,1:T(2,128)(2,1)}), bf16[2,32,10,2048]{3,0,2,1:T(2,128)(2,1)S(1)}, u32[]{:S(2)}, u32[]{:S(2)}) async-start(bf16[2,32,10,2048]{3,0,2,1:T(2,128)(2,1)} %copy.72), calls=%async_computation | async-start | bytes 5242880 | tf_op jit(solution)/shard_map/all_to_all | solution.py:188
  46.1 25.2 %all-gather.16.cloned.1.call-start = ((), (), s32[]{:S(2)}) async-start(), calls=%async_computation.9 | async-start | bytes 1572864 | tf_op jit(solution)/shard_map/all_gather | solution.py:25
  48.1 298.0 %all-gather.18.cloned.1.call-start = ((), (), s32[]{:S(2)}) async-start(), calls=%async_computation.10 | async-start | bytes 1114112 | tf_op jit(solution)/shard_map/all_gather | solution.py:74
  48.9 319.5 %all-gather.12.cloned.1.call-start = ((), (), s32[]{:S(2)}) async-start(), calls=%async_computation.5 | async-start | bytes 8912896 | tf_op jit(solution)/shard_map/all_gather | solution.py:25
  179.0 7.9 %collective-permute-start = (bf16[2,32,10,2048]{3,1,2,0:T(8,128)(2,1)}, bf16[2,32,10,2048]{3,1,2,0:T(8,128)(2,1)}, u32[]{:S(2)}, u32[]{:S(2)}) collective-permute-start(bf16[2,32,10,2048]{3,1,2,0:T(8,128)(2,1)} %copy.73), channel_id=1, source_target_pairs={{0,16},{16,0},{32,48},{48,32},{64,80},{80,64},{96,112},{112,96},{1... | collective-permute-start | bytes 7864328 | tf_op jit(solution)/shard_map/ppermute | solution.py:42
  252.3 2.1 copy-start.22
  252.3 3.1 copy-start.2
  252.3 3.1 copy-start.29
  254.4 2.0 copy-start.10
  255.4 1.0 copy-start.12
  255.4 1.7 copy-start.21
  256.5 0.7 copy-start.27
  256.5 2.2 copy-start.25
  298.9 46.0 %copy-start.15 = (bf16[128,256]{1,0:T(8,128)(2,1)S(1)}, bf16[128,256]{1,0:T(8,128)(2,1)}, u32[]{:S(2)}) copy-start(bf16[128,256]{1,0:T(8,128)(2,1)} %param.22) | copy-start | bytes 196612
  300.0 47.5 %all-to-all-start.2 = ((f32[32,20,128]{2,1,0:T(8,128)}), f32[32,20,128]{2,1,0:T(8,128)S(1)}, u32[]{:S(2)}, u32[]{:S(2)}) async-start(f32[32,20,128]{2,1,0:T(8,128)} %reshape.473), calls=%async_computation.2 | async-start | bytes 786432 | tf_op jit(solution)/shard_map/all_to_all | solution.py:235
  306.9 80.4 %all-gather.14.cloned.1.call-start = ((), (), s32[]{:S(2)}) async-start(), calls=%async_computation.8 | async-start | bytes 3145728 | tf_op jit(solution)/shard_map/all_gather | solution.py:74
  345.1 0.6 copy-start.23
  346.1 73.0 %reduce-scatter.3.cloned.1.call-start = ((), (), s32[]{:S(2)}) async-start(), calls=%async_computation.6 | async-start | bytes 6291456 | tf_op jit(solution)/shard_map/reduce_scatter | solution.py:51
  367.4 1.0 copy-start.7
  368.4 14.7 %copy-start.16 = (bf16[128,256]{1,0:T(8,128)(2,1)S(1)}, bf16[128,256]{1,0:T(8,128)(2,1)}, u32[]{:S(2)}) copy-start(bf16[128,256]{1,0:T(8,128)(2,1)} %param.22) | copy-start | bytes 196612
  368.4 15.5 %copy-start.9 = (bf16[2048,128]{1,0:T(8,128)(2,1)S(1)}, bf16[2048,128]{1,0:T(8,128)(2,1)}, u32[]{:S(2)}) copy-start(bf16[2048,128]{1,0:T(8,128)(2,1)} %copy.77) | copy-start | bytes 1572868
  383.1 0.8 copy-start.5
  387.2 141.9 %all-gather.20.cloned.1.call-start = ((), (), s32[]{:S(2)}) async-start(), calls=%async_computation.11 | async-start | bytes 17301504 | tf_op jit(solution)/shard_map/all_gather | solution.py:89
  389.1 1.8 copy-start.17
  392.4 210.5 %reduce-scatter.5.cloned.1.call-start = ((), (), s32[]{:S(2)}) async-start(), calls=%async_computation.7 | async-start | bytes 2228224 | tf_op jit(solution)/shard_map/reduce_scatter | solution.py:51
  470.1 2.7 copy-start.26
  472.7 1.8 copy-start.3
  472.7 1.8 copy-start.11
  472.7 2.1 copy-start.13
  474.8 1.7 copy-start.20
  474.8 2.0 copy-start.18
  474.8 2.2 copy-start.6
  529.2 71.6 %copy-start.24 = (f32[128,128]{0,1:T(8,128)S(1)}, f32[128,128]{0,1:T(8,128)}, u32[]{:S(2)}) copy-start(f32[128,128]{0,1:T(8,128)} %copy-done.23) | copy-start | bytes 196612
  600.4 2.6 copy-start.1
Sparse Core Ops, SparseCore 0:
  49.5 21.6 all-gather.15
  73.3 96.4 all-gather.17
  172.5 112.8 all-gather.11
  346.2 23.7 all-gather.13
  387.3 31.7 reduce-scatter.2
  421.0 108.0 all-gather.19
  532.5 60.8 reduce-scatter.4
where the time goes:
time: 614 us; the launch traced here: 610 us
  waiting for transfers between devices  201 us (33%)
  blocking collectives  142 us (23%)
  other arithmetic  102 us (17%)
  local copies, waits for them, and re-layouts  90.1 us (15%)
  starting transfers between devices  27.3 us (4%)
  matrix products  26.6 us (4%)
  between operations  18.6 us (3%)
    all_to_all x1, waiting for transfers between devices, local(): lax.all_to_all(packed.reshape(2, seq_devices, half_slots, model_width), S...  102 us
    unnamed x3, blocking collectives  85.4 us
    add x32, other arithmetic, chain_join(): return (earlier[0] * latter[0], latter[0] * earlier[1] + latter[1])  71.2 us
    all_gather x1, waiting for transfers between devices, entering_2(): gathered = jax.tree.map(lambda a: lax.all_gather(a, axis), part)  50.8 us
    all_to_all x1, blocking collectives, local(): lax.all_to_all(partial_in, 'tp', split_axis=1, concat_axis=0, tiled=True)  40.2 us
    slice x1, local copies, waits for them, and re-layouts, local(): cot_rows = received[0]  27.2 us
    reduce_scatter x2, waiting for transfers between devices, reduced_to_own(): pieces = lax.psum_scatter(pieces, axes[k], scatter_dimension=0, tiled=True)  26.6 us
    select_n x1, other arithmetic, local(): jnp.where(is_lower, jnp.concatenate([own_half, partner_half], axis=2), jn...  24.8 us
  transfers between devices with their start and end apart: 10, of which 5 were waited for; matrix products, arithmetic and copies ran while one was open for 32% of the time, Pallas kernels for 0%

commit v1 on v0

v1 whole, which is shorter than its diff:
```python
import functools

import jax
import jax.numpy as jnp
from jax import lax
from jax.experimental import pallas as pl
from jax.experimental.pallas import tpu as pltpu
from jax.sharding import Mesh
from jax.sharding import PartitionSpec as P

SP = ("z", "c")
TP = ("y", "x")
EVERY = ("z", "c", "y", "x")
NORM_EPS = 1.0
SLOTS = 20
PAIR = 2 * SLOTS
BACK = 24
LANES = 128
BF = jnp.bfloat16
F32 = jnp.float32
MESH = pl.DeviceIdType.MESH


def dot(a, b, left=1, right=0):
    return lax.dot_general(a, b, (((left,), (right,)), ((), ())), preferred_element_type=F32)


def iota(shape, dim):
    return lax.broadcasted_iota(jnp.int32, shape, dim)


def moe_kernel(
    nz,
    routes_ref,
    weights_ref,
    cot_hbm,
    stream_hbm,
    gate_hbm,
    up_hbm,
    down_hbm,
    gg_ref,
    gu_ref,
    gd_ref,
    mid_ref,
    wcat,
    down_v,
    cot_s,
    str_s,
    sbuf,
    xs,
    acc,
    wide,
    wide_t,
    gsend,
    gown,
    gpart,
    pbuf,
    pown,
    qbuf,
    tsum,
    town,
    vbuf,
    rsend,
    ret,
    mid_s,
    loc,
    z_s,
    z_r,
    w_s,
    w_r,
    a_s,
    a_r,
    b_s,
    b_r,
    d_s,
    d_r,
    g_s,
    g_r,
    q_s,
    q_r,
    v_s,
    v_r,
    r_s,
    r_r,
    m_s,
    m_r,
):
    z, c, y, x = (lax.axis_index(a) for a in EVERY)
    rows = nz * PAIR
    half = rows // 2
    kept = nz * SLOTS
    t = y * 4 + x

    def peer(da, db):
        py = lax.rem(y + (1 - c) * da + c * db, 4)
        px = lax.rem(x + c * da + (1 - c) * db, 4)
        return (z, c, py, px)

    def tid(da, db):
        _, _, py, px = peer(da, db)
        return py * 4 + px

    def other_tid(da, db):
        py = lax.rem(y + c * da + (1 - c) * db, 4)
        px = lax.rem(x + (1 - c) * da + c * db, 4)
        return py * 4 + px

    def at_z(dz):
        return (lax.rem(z + dz, nz), c, y, x)

    partner = (z, 1 - c, y, x)

    def rc(src, dst, ss, rs, dev):
        return pltpu.make_async_remote_copy(
            src_ref=src, dst_ref=dst, send_sem=ss, recv_sem=rs, device_id=dev, device_id_type=MESH
        )

    barrier = pltpu.get_barrier_semaphore()

    @pl.loop(1, nz)
    def _(dz):
        pl.semaphore_signal(barrier, inc=1, device_id=at_z(dz), device_id_type=MESH)

    @pl.loop(1, 16)
    def _(k):
        pl.semaphore_signal(
            barrier, inc=1, device_id=peer(k // 4, lax.rem(k, 4)), device_id_type=MESH
        )

    pl.semaphore_signal(barrier, inc=1, device_id=partner, device_id_type=MESH)

    cols = pl.ds(pl.multiple_of(t * LANES, LANES), LANES)
    local = [
        pltpu.make_async_copy(cot_hbm.at[:, cols], cot_s, loc.at[0]),
        pltpu.make_async_copy(stream_hbm.at[:, cols], str_s, loc.at[1]),
        pltpu.make_async_copy(gate_hbm, wcat.at[0, :, pl.ds(0, LANES)], loc.at[2]),
        pltpu.make_async_copy(up_hbm, wcat.at[0, :, pl.ds(LANES, LANES)], loc.at[3]),
        pltpu.make_async_copy(down_hbm, down_v, loc.at[4]),
    ]
    for copy in local:
        copy.start()

    experts = iota((nz, LANES), 0)
    named = [(experts == routes_ref[k : k + 1, :]).astype(F32) for k in range(2)]
    before = (iota((LANES, LANES), 0) < iota((LANES, LANES), 1)).astype(BF)
    count = dot((named[0] + named[1]).astype(BF), before)
    rank = [
        jnp.sum(named[k] * count, axis=0, keepdims=True).astype(jnp.int32) for k in range(2)
    ]
    slot = [routes_ref[k : k + 1, :] * PAIR + rank[k] for k in range(2)]
    places = iota((rows, LANES), 0)
    acc[...] = jnp.zeros_like(acc)
    local[0].wait()
    local[1].wait()
    cot = cot_s[...].astype(F32)
    packed = dot(
        jnp.logical_or(places == slot[0] + SLOTS, places == slot[1] + SLOTS).astype(F32).astype(BF),
        str_s[...],
    )
    for k in range(2):
        scaled = (weights_ref[:, k : k + 1] * cot).astype(BF)
        packed = packed + dot((places == slot[k]).astype(F32).astype(BF), scaled)
    sbuf[...] = packed.astype(BF)

    pl.semaphore_wait(barrier, nz - 1 + 15 + 1)

    mine = pl.ds(pl.multiple_of(z * PAIR, 8), PAIR)
    for k in range(1, nz):
        dz = nz // 2 + (k // 2 if k % 2 == 0 else -(k // 2))
        there = pl.ds(pl.multiple_of(lax.rem(z + dz, nz) * PAIR, 8), PAIR)
        rc(sbuf.at[there], xs.at[c, t, mine], z_s.at[dz], z_r.at[dz], at_z(dz)).start()
    own = pltpu.make_async_copy(sbuf.at[mine], xs.at[c, t, mine], loc.at[5])
    own.start()
    local[2].wait()
    local[3].wait()
    weight_copy = rc(wcat.at[0], wcat.at[1], w_s, w_r, partner)
    weight_copy.start()
    local[4].wait()
    own.wait()
    for dz in range(1, nz):
        here = pl.ds(pl.multiple_of(lax.rem(z + nz - dz, nz) * PAIR, 8), PAIR)
        rc(sbuf.at[mine], xs.at[c, t, here], z_s.at[dz], z_r.at[dz], at_z(dz)).wait_recv()

    def product(core, piece):
        a = xs[core, piece]
        deep = pl.ds(pl.multiple_of(piece * LANES, LANES), LANES)
        acc[core, :, 0:256] += dot(a, wcat[0, deep, :])
        acc[core, :, 256:384] += dot(a, down_v[:, deep], 1, 1)

    first = pl.ds(0, half)
    last = pl.ds(half, half)

    def a_copy(k, piece):
        part = (slice(None), slice(None), first, last)[k]
        ref = xs.at[c, piece] if k < 2 else xs.at[c, piece, part]
        return rc(ref, ref, a_s.at[k], a_r.at[k], peer(1 if k % 2 == 0 else 3, 0))

    def b_copy(i, k, piece):
        part = (slice(None), slice(None), first, last)[k]
        ref = xs.at[c, piece] if k < 2 else xs.at[c, piece, part]
        return rc(ref, ref, b_s.at[i, k], b_r.at[i, k], peer(0, 1 if k % 2 == 0 else 3))

    def d_copy(i, j, core, piece):
        ref = xs.at[core, piece]
        return rc(ref, ref, d_s.at[i, j], d_r.at[i, j], partner)

    def spread(i, piece):
        b_copy(i, 0, piece).start()
        b_copy(i, 1, piece).start()
        d_copy(i, 0, c, piece).start()

    a_copy(0, t).start()
    a_copy(1, t).start()
    spread(0, t)
    product(c, t)
    piece = tid(3, 0)
    a_copy(0, piece).wait_recv()
    a_copy(2, piece).start()
    spread(1, piece)
    other = tid(1, 0)
    a_copy(1, other).wait_recv()
    a_copy(3, other).start()
    spread(2, other)
    product(c, piece)
    product(c, other)
    piece = tid(2, 0)
    a_copy(2, piece).wait_recv()
    a_copy(3, piece).wait_recv()
    spread(3, piece)
    product(c, piece)

    def offset(i):
        return (lax.rem(i + 1, 3) + 1) * jnp.minimum(i, 1)

    @pl.loop(0, 4)
    def _(i):
        da = offset(i)
        left, right, far = tid(da, 3), tid(da, 1), tid(da, 2)
        b_copy(i, 0, left).wait_recv()
        b_copy(i, 2, left).start()
        d_copy(i, 1, c, left).start()
        b_copy(i, 1, right).wait_recv()
        b_copy(i, 3, right).start()
        d_copy(i, 2, c, right).start()
        product(c, left)
        product(c, right)
        b_copy(i, 2, far).wait_recv()
        b_copy(i, 3, far).wait_recv()
        d_copy(i, 3, c, far).start()
        product(c, far)
        for j in range(4):
            piece = other_tid(da, (0, 3, 1, 2)[j])
            d_copy(i, j, 1 - c, piece).wait_recv()
            product(1 - c, piece)

    @pl.loop(0, 2 * rows // 80)
    def _(k):
        core = k // (rows // 80)
        at = pl.ds(pl.multiple_of(lax.rem(k, rows // 80) * 80, 8), 80)
        lane_row = iota((80, LANES), 0)
        is_in = jnp.logical_or(
            jnp.logical_and(lane_row >= 20, lane_row < 40), lane_row >= 60
        )
        pre_gate = acc[core, at, 0:128]
        pre_up = acc[core, at, 128:256]
        grad_hidden = pltpu.roll(acc[core, at, 256:384], 20, axis=0)
        gate = jax.nn.sigmoid(pre_gate)
        active = pre_gate * gate
        hidden = active * pre_up
        grad_gate = grad_hidden * pre_up * (gate * (1.0 + pre_gate * (1.0 - gate)))
        grad_up = grad_hidden * active
        wide[core, at, 0:128] = jnp.where(is_in, grad_gate, 0.0).astype(BF)
        wide[core, at, 128:256] = jnp.where(is_in, grad_up, 0.0).astype(BF)
        wide[core, at, 256:384] = jnp.where(is_in, 0.0, pltpu.roll(hidden, 60, axis=0)).astype(BF)

    low = iota((kept, rows), 0)
    pick = (iota((kept, rows), 1) == low + SLOTS * ((low * 3277) // 65536) + SLOTS)
    pick = pick.astype(F32).astype(BF)
    gsend[...] = dot(pick, wide[1 - c, :, 0:256]).astype(BF)
    grad_copy = rc(gsend, gpart, g_s, g_r, partner)
    grad_copy.start()
    gown[...] = dot(pick, wide[c, :, 0:256]).astype(BF)
    weight_copy.wait_recv()
    grad_copy.wait_recv()

    def partial_in(piece):
        deep = pl.ds(pl.multiple_of(piece * LANES, LANES), LANES)
        return dot(gown[...], wcat[0, deep, :], 1, 1) + dot(gpart[...], wcat[1, deep, :], 1, 1)

    def q_copy(da):
        return rc(pbuf.at[da - 1], qbuf.at[da - 1], q_s.at[da - 1], q_r.at[da - 1], peer(da, 0))

    for da in (2, 1, 3):

        @pl.loop(0, 4)
        def _(db):
            pbuf[da - 1, db] = partial_in(tid(da, db)).astype(BF)

        q_copy(da).start()

    @pl.loop(0, 4)
    def _(db):
        pown[db] = partial_in(tid(0, db))

    for core in range(2):
        wide_t[core] = wide[core].T

    @pl.loop(0, 16)
    def _(piece):
        deep = pl.ds(pl.multiple_of(piece * LANES, LANES), LANES)
        total = dot(wide_t[0], xs[0, piece]) + dot(wide_t[1], xs[1, piece])
        gd_ref[:, deep] = total[256:384].astype(BF)
        gg_ref[deep, :] = total[0:128].T.astype(BF)
        gu_ref[deep, :] = total[128:256].T.astype(BF)

    for da in (1, 3, 2):
        q_copy(da).wait_recv()

    def v_copy(db):
        return rc(tsum.at[db - 1], vbuf.at[db - 1], v_s.at[db - 1], v_r.at[db - 1], peer(0, db))

    for db in (2, 1, 3):
        whole = pown[db]
        for da in range(3):
            whole = whole + qbuf[da, db].astype(F32)
        tsum[db - 1] = whole.astype(BF)
        v_copy(db).start()
    whole = pown[0]
    for da in range(3):
        whole = whole + qbuf[da, 0].astype(F32)
    town[...] = whole
    for db in (1, 3, 2):
        v_copy(db).wait_recv()
    whole = town[...]
    for db in range(3):
        whole = whole + vbuf[db].astype(F32)
    low = iota((nz * BACK, kept), 0)
    block = (low * 2731) // 65536
    spreadm = jnp.logical_and(
        iota((nz * BACK, kept), 1) == low - (BACK - SLOTS) * block, low - BACK * block < SLOTS
    )
    rsend[...] = dot(spreadm.astype(F32).astype(BF), whole.astype(BF)).astype(BF)

    here = pl.ds(pl.multiple_of(z * BACK, 8), BACK)
    for k in range(1, nz):
        dz = nz // 2 + (k // 2 if k % 2 == 0 else -(k // 2))
        there = pl.ds(pl.multiple_of(lax.rem(z + dz, nz) * BACK, 8), BACK)
        rc(rsend.at[there], ret.at[here], r_s.at[dz], r_r.at[dz], at_z(dz)).start()
    own = pltpu.make_async_copy(rsend.at[here], ret.at[here], loc.at[6])
    own.start()
    places = iota((nz * BACK, LANES), 0)
    take = jnp.logical_or(
        places == routes_ref[0:1, :] * BACK + rank[0], places == routes_ref[1:2, :] * BACK + rank[1]
    )
    take = take.astype(F32).astype(BF)
    own.wait()
    for dz in range(1, nz):
        there = pl.ds(pl.multiple_of(lax.rem(z + nz - dz, nz) * BACK, 8), BACK)
        rc(rsend.at[here], ret.at[there], r_s.at[dz], r_r.at[dz], at_z(dz)).wait_recv()
    mid_s[:, cols] = (cot_s[...].astype(F32) + dot(take, ret[...], 0, 0)).astype(BF)

    @pl.loop(1, 16)
    def _(k):
        dev = peer(k // 4, lax.rem(k, 4))
        rc(mid_s.at[:, cols], mid_s.at[:, cols], m_s.at[k], m_r.at[k], dev).start()

    @pl.loop(1, 16)
    def _(k):
        back = tid(lax.rem(4 - k // 4, 4), lax.rem(4 - lax.rem(k, 4), 4))
        theirs = pl.ds(pl.multiple_of(back * LANES, LANES), LANES)
        dev = peer(k // 4, lax.rem(k, 4))
        rc(mid_s.at[:, cols], mid_s.at[:, theirs], m_s.at[k], m_r.at[k], dev).wait_recv()

    mid_ref[...] = mid_s[...]

    for dz in range(1, nz):
        rc(sbuf.at[mine], xs.at[c, t, mine], z_s.at[dz], z_r.at[dz], at_z(dz)).wait_send()
        rc(rsend.at[here], ret.at[here], r_s.at[dz], r_r.at[dz], at_z(dz)).wait_send()
    weight_copy.wait_send()
    grad_copy.wait_send()
    for k in range(4):
        a_copy(k, t).wait_send()

    @pl.loop(0, 4)
    def _(i):
        for k in range(4):
            b_copy(i, k, t).wait_send()
            d_copy(i, k, c, t).wait_send()

    for k in range(1, 4):
        q_copy(k).wait_send()
        v_copy(k).wait_send()

    @pl.loop(1, 16)
    def _(k):
        dev = peer(k // 4, lax.rem(k, 4))
        rc(mid_s.at[:, cols], mid_s.at[:, cols], m_s.at[k], m_r.at[k], dev).wait_send()


def moe(nz, routes, route_weights, cotangent, stream, gate, up, down):
    width = cotangent.shape[1]
    rows, kept = nz * PAIR, nz * SLOTS
    any_ = pl.BlockSpec(memory_space=pl.ANY)
    vmem = pl.BlockSpec(memory_space=pltpu.VMEM)
    dma = pltpu.SemaphoreType.DMA
    return pl.pallas_call(
        functools.partial(moe_kernel, nz),
        out_shape=(
            jax.ShapeDtypeStruct((width, LANES), BF),
            jax.ShapeDtypeStruct((width, LANES), BF),
            jax.ShapeDtypeStruct((LANES, width), BF),
            jax.ShapeDtypeStruct((LANES, width), BF),
        ),
        in_specs=[vmem, vmem, any_, any_, any_, any_, any_],
        out_specs=(vmem,) * 4,
        scratch_shapes=[
            pltpu.VMEM((2, width, 2 * LANES), BF),
            pltpu.VMEM((LANES, width), BF),
            pltpu.VMEM((LANES, LANES), BF),
            pltpu.VMEM((LANES, LANES), BF),
            pltpu.VMEM((rows, LANES), BF),
            pltpu.VMEM((2, 16, rows, LANES), BF),
            pltpu.VMEM((2, rows, 3 * LANES), F32),
            pltpu.VMEM((2, rows, 3 * LANES), BF),
            pltpu.VMEM((2, 3 * LANES, rows), BF),
            pltpu.VMEM((kept, 2 * LANES), BF),
            pltpu.VMEM((kept, 2 * LANES), BF),
            pltpu.VMEM((kept, 2 * LANES), BF),
            pltpu.VMEM((3, 4, kept, LANES), BF),
            pltpu.VMEM((4, kept, LANES), F32),
            pltpu.VMEM((3, 4, kept, LANES), BF),
            pltpu.VMEM((3, kept, LANES), BF),
            pltpu.VMEM((kept, LANES), F32),
            pltpu.VMEM((3, kept, LANES), BF),
            pltpu.VMEM((nz * BACK, LANES), BF),
            pltpu.VMEM((nz * BACK, LANES), BF),
            pltpu.VMEM((LANES, width), BF),
            dma((7,)),
            dma((nz,)),
            dma((nz,)),
            dma,
            dma,
            dma((4,)),
            dma((4,)),
            dma((4, 4)),
            dma((4, 4)),
            dma((4, 4)),
            dma((4, 4)),
            dma,
            dma,
            dma((3,)),
            dma((3,)),
            dma((3,)),
            dma((3,)),
            dma((nz,)),
            dma((nz,)),
            dma((16,)),
            dma((16,)),
        ],
        compiler_params=pltpu.CompilerParams(
            collective_id=0, has_side_effects=True, vmem_limit_bytes=56 * 2**20
        ),
        cost_estimate=pl.CostEstimate(flops=60_000_000_000, bytes_accessed=0, transcendentals=0),
        name="moe",
    )(routes.T, route_weights, cotangent, stream, gate, up, down)


def owner_scan(state, weights):
    parts = weights.shape[0]
    piece = state.astype(BF).reshape(parts, -1, state.shape[1])
    piece = lax.all_to_all(piece, SP, 0, 0, tiled=True)
    mixed = jnp.einsum(
        "bj,jxy->bxy", weights, piece.astype(F32), precision=lax.Precision.HIGHEST
    ).astype(BF)
    return lax.all_to_all(mixed, SP, 0, 0, tiled=True).reshape(state.shape)


def local(
    cotangent,
    stream,
    routes,
    route_weights,
    gate_proj,
    up_proj,
    down_proj,
    out_weight,
    queries,
    keys,
    values,
    decay_rate,
):
    nz = lax.axis_size("z")
    blocks = 2 * nz
    tok_rows = cotangent.shape[0]
    rate = decay_rate[0]
    steps = jnp.arange(tok_rows, dtype=F32)
    distance = steps[:, None] - steps[None, :]
    mask = jnp.where(distance >= 0, jnp.exp(-rate * jnp.maximum(distance, 0.0)), 0.0)
    enter = jnp.exp(-rate * (steps + 1.0))[:, None]
    leave = jnp.exp(-rate * (tok_rows - 1.0 - steps))[:, None]
    start = jnp.exp(-rate * steps)[:, None]
    trail = jnp.exp(-rate * (tok_rows - steps))[:, None]
    order = jnp.arange(blocks, dtype=F32)
    apart = order[:, None] - order[None, :] - 1.0
    earlier = jnp.where(apart >= 0, jnp.exp(-rate * tok_rows * jnp.maximum(apart, 0.0)), 0.0)
    later = earlier.T
    keys = keys * BF(keys.shape[1] ** -0.5)
    key_wide = keys.astype(F32)
    query_wide = queries.astype(F32)
    carried = owner_scan(dot((key_wide * leave).astype(BF), values, 0, 0), earlier)
    scores = dot(queries, keys, 1, 1) * mask
    scores_b = scores.astype(BF)
    retained = dot(scores_b, values) + enter * dot(queries, carried)
    centered = retained - jnp.mean(retained, axis=-1, keepdims=True)
    inv_scale = lax.rsqrt(jnp.mean(centered * centered, axis=-1, keepdims=True) + NORM_EPS)
    normed = centered * inv_scale
    mixed = normed.astype(BF)
    weight = lax.all_gather(out_weight, SP, axis=0, tiled=True)

    grad_gate, grad_up, grad_down, mid_grad = moe(
        nz, routes, route_weights, cotangent, stream, gate_proj[0], up_proj[0], down_proj[0]
    )

    head_grad = dot(mid_grad, weight)
    grad_out_weight = dot(mid_grad, mixed, 0, 0)
    for axis in SP:
        grad_out_weight = lax.psum_scatter(grad_out_weight, axis, scatter_dimension=0, tiled=True)
    grad_retained = inv_scale * (
        head_grad
        - jnp.mean(head_grad, axis=-1, keepdims=True)
        - normed * jnp.mean(head_grad * normed, axis=-1, keepdims=True)
    )
    ret_b = grad_retained.astype(BF)
    future = owner_scan(dot((query_wide * start).astype(BF), ret_b, 0, 0), later)
    score_grad = (dot(ret_b, values, 1, 1) * mask).astype(BF)
    grad_queries = dot(score_grad, keys) + enter * dot(ret_b, carried, 1, 1)
    grad_keys = (
        dot(score_grad, queries, 0, 0) + trail * dot(values, future, 1, 1)
    ) * queries.shape[1] ** (-0.5)
    grad_values = dot(scores_b, ret_b, 0, 0) + trail * dot(keys, future)
    return (
        grad_gate[None],
        grad_up[None],
        grad_down[None],
        grad_out_weight,
        grad_queries.astype(BF),
        grad_keys.astype(BF),
        grad_values.astype(BF),
    )


def solution(mesh):
    blocks, heads = mesh.devices.shape
    split = Mesh(mesh.devices.reshape(blocks // 2, 2, 4, heads // 4), EVERY)
    tokens = P(SP, None)
    tiles = P(SP, TP)
    in_specs = (
        tokens,
        tokens,
        tokens,
        tokens,
        P(SP, None, TP),
        P(SP, None, TP),
        P(SP, TP, None),
        tiles,
        tiles,
        tiles,
        tiles,
        P(TP),
    )
    out_specs = (
        P(SP, None, TP),
        P(SP, None, TP),
        P(SP, TP, None),
        tiles,
        tiles,
        tiles,
        tiles,
    )
    return jax.shard_map(local, mesh=split, in_specs=in_specs, out_specs=out_specs, check_vma=False)
```

time: 614 us -> 288 us (0.47)
  blocking collectives: 142 us -> 0 us
  Pallas kernels: 0 us -> 103 us
  other arithmetic: 102 us -> 0.39 us
  waiting for transfers between devices: 201 us -> 115 us
  local copies, waits for them, and re-layouts: 90.1 us -> 5.86 us
  matrix products: 26.6 us -> 12.5 us
  starting transfers between devices: 27.3 us -> 34.5 us
    pallas_call x0 -> x1, Pallas kernels: none -> 103 us  [moe(): pl.pallas_call(functools.partial(moe_kernel, nz), out_shape=(jax.ShapeDty...]
    unnamed x3 -> x0, blocking collectives: 85.4 us -> none
    add x34 -> x0, other arithmetic: 71.9 us -> none  [the longest x32 71.2 us: chain_join(): return (earlier[0] * latter[0], latter[0] * earlier[1] + latter[1])]
    all_gather x5 -> x1, waiting for transfers between devices: 67.4 us -> 0.02 us  [local(): weight = lax.all_gather(out_weight, SP, axis=0, tiled=True)]
    all_to_all x2 -> x4, waiting for transfers between devices: 102 us -> 45.2 us  [the longest x2 45.2 us: owner_scan(): piece = lax.all_to_all(piece, SP, 0, 0, tiled=True)]
    reduce_scatter x2, waiting for transfers between devices: 26.6 us -> 69.5 us  [local(): lax.psum_scatter(grad_out_weight, axis, scatter_dimension=0, tiled=True)]
    all_to_all x1 -> x0, blocking collectives: 40.2 us -> none  [local(): lax.all_to_all(partial_in, 'tp', split_axis=1, concat_axis=0, tiled=True)]
    slice x4 -> x0, local copies, waits for them, and re-layouts: 28.7 us -> none  [the longest x1 27.2 us: local(): cot_rows = received[0]]
  transfers between devices with their start and end apart: 10 -> 7, of which waited for: 5 -> 4; matrix products, arithmetic and copies ran while one was open for 32% -> 5% of each run, Pallas kernels for 0% -> 36%
where the time goes in v1:
time: 288 us
  waiting for transfers between devices  115 us (40%)
  Pallas kernels  103 us (36%)
  starting transfers between devices  34.5 us (12%)
  between operations  16.4 us (6%)
  matrix products  12.5 us (4%)
  local copies, waits for them, and re-layouts  5.86 us (2%)
    pallas_call x1, Pallas kernels, moe(): pl.pallas_call(functools.partial(moe_kernel, nz), out_shape=(jax.ShapeDty...  103 us
    reduce_scatter x2, waiting for transfers between devices, local(): lax.psum_scatter(grad_out_weight, axis, scatter_dimension=0, tiled=True)  69.5 us
    all_to_all x2, waiting for transfers between devices, owner_scan(): piece = lax.all_to_all(piece, SP, 0, 0, tiled=True)  45.2 us
    all_to_all x2, starting transfers between devices, owner_scan(): piece = lax.all_to_all(piece, SP, 0, 0, tiled=True)  26 us
    dot_general x14, matrix products, dot(): lax.dot_general(a, b, (((left,), (right,)), ((), ())), preferred_element_...  11.6 us
    all_to_all x2, starting transfers between devices, owner_scan(): return lax.all_to_all(mixed, SP, 0, 0, tiled=True).reshape(state.shape)  8.4 us
  transfers between devices with their start and end apart: 7, of which 4 were waited for; matrix products, arithmetic and copies ran while one was open for 5% of the time, Pallas kernels for 36%

profile of v1, /device:TPU:1, one launch (start us, length us, event | category | flops | bytes accessed | tf_op | source)
XLA Modules:
  0.0 287.8 jit_solution(10977324623875564707)
XLA Ops:
  8.0 0.0 copy-start
  8.7 0.2 copy-done
  8.9 1.9 fusion.3
  10.8 16.7 %all-to-all-start = ((bf16[32,8,512]{2,1,0:T(8,128)(2,1)}), bf16[32,8,512]{2,1,0:T(8,128)(2,1)S(1)}, u32[]{:S(2)}, u32[]{:S(2)}) async-start(bf16[32,8,512]{2,1,0:T(8,128)(2,1)} %fusion.3), calls=%async_computation | async-start | bytes 524288 | tf_op jit(solution)/shard_map/all_to_all | solution.py:471
  27.5 0.0 all-gather.2.cloned.1.call-start
  27.6 0.7 all-gather.2.cloned.1.call-update
  28.3 1.4 copy.35.weights_ref
  29.7 20.1 %all-to-all-done = bf16[32,8,512]{2,1,0:T(8,128)(2,1)S(1)} async-done(((bf16[32,8,512]{2,1,0:T(8,128)(2,1)}), bf16[32,8,512]{2,1,0:T(8,128)(2,1)S(1)}, u32[]{:S(2)}, u32[]{:S(2)}) %all-to-all-start) | async-done | bytes 262176 | tf_op jit(solution)/shard_map/all_to_all | solution.py:471
  49.8 0.4 convolution_convert_fusion.2
  50.2 0.9 copy.38
  51.1 4.2 %all-to-all-start.1 = ((bf16[32,8,512]{2,1,0:T(8,128)(2,1)}), bf16[32,8,512]{2,1,0:T(8,128)(2,1)S(1)}, u32[]{:S(2)}, u32[]{:S(2)}) async-start(bf16[32,8,512]{2,1,0:T(8,128)(2,1)} %copy.38), calls=%async_computation.1 | async-start | bytes 524288 | tf_op jit(solution)/shard_map/all_to_all | solution.py:475
  55.3 0.0 reduce-scatter.3.cloned.1.call-start
  55.3 0.0 copy-start.2
  55.3 0.0 copy-start.3
  55.3 102.8 %moe.1 = (bf16[2048,128]{1,0:T(8,128)(2,1)}, bf16[2048,128]{1,0:T(8,128)(2,1)}, bf16[128,2048]{1,0:T(8,128)(2,1)}, bf16[128,2048]{1,0:T(8,128)(2,1)}) custom-call(s32[2,128]{1,0:T(2,128)} %bitcast.72, f32[128,2]{1,0:T(8,128)} %copy.35.weights_ref, bf16[128,2048]{1,0:T(8,128)(2,1)} %cot_hbm.1, bf16[128,2048]{1,0:T(8,128)(2,1)} %stream_hbm.1, ...), custom_call_target="tpu_custom_call" | custom-call | flops 60000002048 | tf_op jit(solution)/shard_map/moe/pallas_call | solution.py:406
  158.1 0.0 copy-start.1
  158.2 0.2 fusion.13
  158.3 0.2 fusion.59
  158.5 0.0 all-to-all-done.1
  158.6 0.3 fusion.58
  158.8 0.2 multiply_reduce_fusion.1
  159.0 0.1 copy-done.1
  159.2 2.7 fusion.22
  161.9 0.0 reduce-scatter.3.cloned.1.call-update
  161.9 0.0 all-gather.2.cloned.1.call-done
  162.0 2.1 fusion.57
  164.1 0.1 multiply_convert_fusion
  164.2 1.0 fusion.4
  165.3 9.3 %all-to-all-start.2 = ((bf16[32,8,512]{2,1,0:T(8,128)(2,1)}), bf16[32,8,512]{2,1,0:T(8,128)(2,1)S(1)}, u32[]{:S(2)}, u32[]{:S(2)}) async-start(bf16[32,8,512]{2,1,0:T(8,128)(2,1)} %fusion.4), calls=%async_computation.4 | async-start | bytes 524288 | tf_op jit(solution)/shard_map/all_to_all | solution.py:471
  174.6 25.0 %all-to-all-done.2 = bf16[32,8,512]{2,1,0:T(8,128)(2,1)S(1)} async-done(((bf16[32,8,512]{2,1,0:T(8,128)(2,1)}), bf16[32,8,512]{2,1,0:T(8,128)(2,1)S(1)}, u32[]{:S(2)}, u32[]{:S(2)}) %all-to-all-start.2) | async-done | bytes 262176 | tf_op jit(solution)/shard_map/all_to_all | solution.py:471
  199.6 0.4 convolution_convert_fusion
  200.0 0.9 copy.42
  200.9 4.2 %all-to-all-start.3 = ((bf16[32,8,512]{2,1,0:T(8,128)(2,1)}), bf16[32,8,512]{2,1,0:T(8,128)(2,1)S(1)}, u32[]{:S(2)}, u32[]{:S(2)}) async-start(bf16[32,8,512]{2,1,0:T(8,128)(2,1)} %copy.42), calls=%async_computation.5 | async-start | bytes 524288 | tf_op jit(solution)/shard_map/all_to_all | solution.py:475
  205.1 0.0 reduce-scatter.5.cloned.1.call-start
  205.1 0.2 fusion.14
  205.3 0.2 fusion.30
  205.5 0.2 fusion.61
  205.7 0.9 fusion.10
  206.6 42.5 %reduce-scatter.3.cloned.1.call-done = f32[128,512]{1,0:T(8,128)} async-done(((f32[2048,512]{1,0:T(8,128)}), f32[128,512]{1,0:T(8,128)}) %reduce-scatter.3.cloned.1.call-update) | async-done | bytes 262160 | tf_op jit(solution)/shard_map/reduce_scatter | solution.py:527
  249.1 0.0 reduce-scatter.5.cloned.1.call-update
  249.1 0.1 fusion.60
  249.3 0.0 all-to-all-done.3
  249.3 0.9 fusion.11
  250.1 0.8 fusion.5
  251.0 27.0 %reduce-scatter.5.cloned.1.call-done = f32[64,512]{1,0:T(8,128)} async-done(((f32[128,512]{1,0:T(8,128)}), f32[64,512]{1,0:T(8,128)}) %reduce-scatter.5.cloned.1.call-update) | async-done | bytes 131088 | tf_op jit(solution)/shard_map/reduce_scatter | solution.py:527
  278.0 0.8 copy.57
  278.8 0.8 copy.58
  279.6 0.8 copy.59
  (15 shorter events, 0.1 us)
Async XLA Ops:
  8.0 0.9 copy-start
  10.8 39.0 %all-to-all-start = ((bf16[32,8,512]{2,1,0:T(8,128)(2,1)}), bf16[32,8,512]{2,1,0:T(8,128)(2,1)S(1)}, u32[]{:S(2)}, u32[]{:S(2)}) async-start(bf16[32,8,512]{2,1,0:T(8,128)(2,1)} %fusion.3), calls=%async_computation | async-start | bytes 524288 | tf_op jit(solution)/shard_map/all_to_all | solution.py:471
  27.5 134.4 %all-gather.2.cloned.1.call-start = ((), (), s32[]{:S(2)}) async-start(), calls=%async_computation.8 | async-start | bytes 2162688 | tf_op jit(solution)/shard_map/all_gather | solution.py:518
  51.1 107.5 %all-to-all-start.1 = ((bf16[32,8,512]{2,1,0:T(8,128)(2,1)}), bf16[32,8,512]{2,1,0:T(8,128)(2,1)S(1)}, u32[]{:S(2)}, u32[]{:S(2)}) async-start(bf16[32,8,512]{2,1,0:T(8,128)(2,1)} %copy.38), calls=%async_computation.1 | async-start | bytes 524288 | tf_op jit(solution)/shard_map/all_to_all | solution.py:475
  55.3 193.8 %reduce-scatter.3.cloned.1.call-start = ((), (), s32[]{:S(2)}) async-start(), calls=%async_computation.6 | async-start | bytes 4456448 | tf_op jit(solution)/shard_map/reduce_scatter | solution.py:527
  55.3 102.8 %copy-start.2 = (bf16[128,256]{1,0:T(8,128)(2,1)S(1)}, bf16[128,256]{1,0:T(8,128)(2,1)}, u32[]{:S(2)}) copy-start(bf16[128,256]{1,0:T(8,128)(2,1)} %param.21) | copy-start | bytes 196612
  55.3 102.8 %copy-start.3 = (bf16[128,256]{1,0:T(8,128)(2,1)S(1)}, bf16[128,256]{1,0:T(8,128)(2,1)}, u32[]{:S(2)}) copy-start(bf16[128,256]{1,0:T(8,128)(2,1)} %param.20) | copy-start | bytes 196612
  158.1 1.0 copy-start.1
  165.3 34.3 %all-to-all-start.2 = ((bf16[32,8,512]{2,1,0:T(8,128)(2,1)}), bf16[32,8,512]{2,1,0:T(8,128)(2,1)S(1)}, u32[]{:S(2)}, u32[]{:S(2)}) async-start(bf16[32,8,512]{2,1,0:T(8,128)(2,1)} %fusion.4), calls=%async_computation.4 | async-start | bytes 524288 | tf_op jit(solution)/shard_map/all_to_all | solution.py:471
  200.0 78.0 %copy-start.6 = (bf16[2048,128]{1,0:T(8,128)(2,1)S(1)}, bf16[2048,128]{1,0:T(8,128)(2,1)}, u32[]{:S(2)}) copy-start(bf16[2048,128]{1,0:T(8,128)(2,1)} %get-tuple-element.11) | copy-start | bytes 1572868
  200.9 48.4 %all-to-all-start.3 = ((bf16[32,8,512]{2,1,0:T(8,128)(2,1)}), bf16[32,8,512]{2,1,0:T(8,128)(2,1)S(1)}, u32[]{:S(2)}, u32[]{:S(2)}) async-start(bf16[32,8,512]{2,1,0:T(8,128)(2,1)} %copy.42), calls=%async_computation.5 | async-start | bytes 524288 | tf_op jit(solution)/shard_map/all_to_all | solution.py:475
  205.1 72.9 %reduce-scatter.5.cloned.1.call-start = ((), (), s32[]{:S(2)}) async-start(), calls=%async_computation.7 | async-start | bytes 393216 | tf_op jit(solution)/shard_map/reduce_scatter | solution.py:527
  205.3 73.5 %copy-start.5 = (bf16[2048,128]{1,0:T(8,128)(2,1)S(1)}, bf16[2048,128]{1,0:T(8,128)(2,1)}, u32[]{:S(2)}) copy-start(bf16[2048,128]{1,0:T(8,128)(2,1)} %get-tuple-element.12) | copy-start | bytes 1572868
  206.6 73.0 %copy-start.4 = (bf16[128,2048]{1,0:T(8,128)(2,1)S(1)}, bf16[128,2048]{1,0:T(8,128)(2,1)}, u32[]{:S(2)}) copy-start(bf16[128,2048]{1,0:T(8,128)(2,1)} %get-tuple-element.13) | copy-start | bytes 1572868
Sparse Core Ops, SparseCore 0:
  30.5 78.5 all-gather.1
Sparse Core Ops, SparseCore 1:
  162.0 87.1 reduce-scatter.2
  252.3 25.6 reduce-scatter.4

commit v2 on v1

--- a/solution.py
+++ b/solution.py
@@ -29,7 +29,7 @@
     return lax.broadcasted_iota(jnp.int32, shape, dim)
 
 
-def moe_kernel(
+def kernel(
     nz,
     routes_ref,
     weights_ref,
@@ -38,10 +38,18 @@
     gate_hbm,
     up_hbm,
     down_hbm,
+    out_weight_hbm,
+    q_ref,
+    k_ref,
+    v_ref,
+    rate_ref,
     gg_ref,
     gu_ref,
     gd_ref,
-    mid_ref,
+    gow_ref,
+    gq_ref,
+    gk_ref,
+    gv_ref,
     wcat,
     down_v,
     cot_s,
@@ -62,7 +70,27 @@
     vbuf,
     rsend,
     ret,
-    mid_s,
+    mids,
+    wfull,
+    state,
+    half_state,
+    slices,
+    scanned,
+    carried,
+    mixes,
+    scores,
+    norm_s,
+    inv_s,
+    back_state,
+    half_back,
+    bslices,
+    bscanned,
+    future,
+    prods,
+    up_s,
+    up_r,
+    dn_s,
+    dn_r,
     loc,
     z_s,
     z_r,
@@ -84,6 +112,18 @@
     r_r,
     m_s,
     m_r,
+    wr_s,
+    wr_r,
+    wd_s,
+    wd_r,
+    x_s,
+    x_r,
+    f_s,
+    f_r,
+    h_s,
+    h_r,
+    o_s,
+    o_r,
 ):
     z, c, y, x = (lax.axis_index(a) for a in EVERY)
     rows = nz * PAIR
@@ -114,6 +154,42 @@
         return pltpu.make_async_remote_copy(
             src_ref=src, dst_ref=dst, send_sem=ss, recv_sem=rs, device_id=dev, device_id_type=MESH
         )
+
+    def at_other(dz):
+        return (lax.rem(z + dz, nz), 1 - c, y, x)
+
+    def w_rows(dz, core):
+        return pl.ds(pl.multiple_of((lax.rem(z + dz, nz) * 2 + core) * 64, 64), 64)
+
+    rate = rate_ref[0]
+    down = nz - 1
+
+    def ring(way, s):
+        dz = (nz - s + 1) if way == 0 else (s - 1)
+        ref = wfull.at[w_rows(dz, c)]
+        return rc(ref, ref, wr_s.at[way, s], wr_r.at[way, s], at_z(1 if way == 0 else down))
+
+    def ring_got(way, s):
+        dz = nz - s if way == 0 else s
+        ref = wfull.at[w_rows(dz, c)]
+        return rc(ref, ref, wr_s.at[way, s], wr_r.at[way, s], at_z(1 if way == 0 else down))
+
+    def pass_on(dz, core):
+        ref = wfull.at[w_rows(dz, core)]
+        return rc(ref, ref, wd_s.at[dz], wd_r.at[dz], partner)
+
+    far = nz // 2
+
+    def ring_step(s):
+        ring_got(0, s).wait_recv()
+        if s < far:
+            ring(0, s + 1).start()
+        pass_on(nz - s, c).start()
+        if s < far:
+            ring_got(1, s).wait_recv()
+            if s < far - 1:
+                ring(1, s + 1).start()
+            pass_on(s, c).start()
 
     barrier = pltpu.get_barrier_semaphore()
 
@@ -136,6 +212,7 @@
         pltpu.make_async_copy(gate_hbm, wcat.at[0, :, pl.ds(0, LANES)], loc.at[2]),
         pltpu.make_async_copy(up_hbm, wcat.at[0, :, pl.ds(LANES, LANES)], loc.at[3]),
         pltpu.make_async_copy(down_hbm, down_v, loc.at[4]),
+        pltpu.make_async_copy(out_weight_hbm, wfull.at[w_rows(0, c)], loc.at[7]),
     ]
     for copy in local:
         copy.start()
@@ -171,6 +248,33 @@
         rc(sbuf.at[there], xs.at[c, t, mine], z_s.at[dz], z_r.at[dz], at_z(dz)).start()
     own = pltpu.make_async_copy(sbuf.at[mine], xs.at[c, t, mine], loc.at[5])
     own.start()
+    steps = iota((LANES, 1), 0).astype(F32)
+    scale = k_ref.shape[1] ** -0.5
+    block_decay = jnp.exp(-rate * jnp.full((1, 512), float(LANES), F32))
+    chip_decay = jnp.exp(-rate * jnp.full((1, 512), 2.0 * LANES, F32))
+    keys = (k_ref[...].astype(F32) * scale).astype(BF)
+    vals = v_ref[...]
+
+    def split(a):
+        high = a.astype(BF)
+        return high, (a - high.astype(F32)).astype(BF)
+
+    def dot2(a, b, left=1, right=0):
+        high, low = split(a)
+        return dot(high, b, left, right) + dot(low, b, left, right)
+
+    def dot_2(a, b, left=1, right=0):
+        high, low = split(b)
+        return dot(a, high, left, right) + dot(a, low, left, right)
+
+    leave = jnp.exp(-rate * (LANES - 1.0 - steps))
+    state[c] = dot2(keys.astype(F32) * leave, vals, 0, 0)
+    state_copy = rc(state.at[c], state.at[c], x_s.at[0], x_r.at[0], partner)
+    state_copy.start()
+    local[5].wait()
+    ring(0, 1).start()
+    ring(1, 1).start()
+    pass_on(0, c).start()
     local[2].wait()
     local[3].wait()
     weight_copy = rc(wcat.at[0], wcat.at[1], w_s, w_r, partner)
@@ -228,6 +332,34 @@
     a_copy(3, piece).wait_recv()
     spread(3, piece)
     product(c, piece)
+
+    rows_here = pl.ds(pl.multiple_of(c * 128, 128), 128)
+    rows_there = pl.ds(pl.multiple_of((1 - c) * 128, 128), 128)
+
+    def slice_of(dz):
+        return pl.ds(pl.multiple_of(lax.rem(z + dz, nz) * 8, 8), 8)
+
+    def exchange(src, dst, ss, rs):
+        for k in range(1, nz):
+            dz = nz // 2 + (k // 2 if k % 2 == 0 else -(k // 2))
+            rc(src.at[slice_of(dz)], dst.at[slice_of(0)], ss.at[dz], rs.at[dz], at_z(dz)).start()
+        mine_copy = pltpu.make_async_copy(src.at[slice_of(0)], dst.at[slice_of(0)], ss.at[0])
+        mine_copy.start()
+
+    def exchanged(src, dst, ss, rs):
+        pltpu.make_async_copy(src.at[slice_of(0)], dst.at[slice_of(0)], ss.at[0]).wait()
+        for dz in range(1, nz):
+            rc(
+                src.at[slice_of(0)], dst.at[slice_of(nz - dz)], ss.at[dz], rs.at[dz], at_z(dz)
+            ).wait_recv()
+
+    def exchange_sent(src, dst, ss, rs):
+        for dz in range(1, nz):
+            rc(src.at[slice_of(0)], dst.at[slice_of(0)], ss.at[dz], rs.at[dz], at_z(dz)).wait_send()
+
+    rc(state.at[1 - c], state.at[1 - c], x_s.at[0], x_r.at[0], partner).wait_recv()
+    half_state[...] = block_decay * state[0, rows_here, :] + state[1, rows_here, :]
+    exchange(half_state, slices, f_s.at[0], f_r.at[0])
 
     def offset(i):
         return (lax.rem(i + 1, 3) + 1) * jnp.minimum(i, 1)
@@ -252,6 +384,10 @@
             piece = other_tid(da, (0, 3, 1, 2)[j])
             d_copy(i, j, 1 - c, piece).wait_recv()
             product(1 - c, piece)
+        for s in range(1, 5):
+            @pl.when(i == s - 1)
+            def _():
+                ring_step(s)
 
     @pl.loop(0, 2 * rows // 80)
     def _(k):
@@ -273,6 +409,14 @@
         wide[core, at, 128:256] = jnp.where(is_in, grad_up, 0.0).astype(BF)
         wide[core, at, 256:384] = jnp.where(is_in, 0.0, pltpu.roll(hidden, 60, axis=0)).astype(BF)
 
+    exchanged(half_state, slices, f_s.at[0], f_r.at[0])
+    running = jnp.zeros((8, 512), F32)
+    for e in range(nz):
+        scanned[e * 8 : e * 8 + 8, :] = running
+        running = chip_decay * running + slices[e * 8 : e * 8 + 8, :]
+    exchange(scanned, carried.at[rows_here], f_s.at[1], f_r.at[1])
+    ring_step(5)
+
     low = iota((kept, rows), 0)
     pick = (iota((kept, rows), 1) == low + SLOTS * ((low * 3277) // 65536) + SLOTS)
     pick = pick.astype(F32).astype(BF)
@@ -302,6 +446,8 @@
     def _(db):
         pown[db] = partial_in(tid(0, db))
 
+    ring_step(6)
+
     for core in range(2):
         wide_t[core] = wide[core].T
 
@@ -313,6 +459,7 @@
         gg_ref[deep, :] = total[0:128].T.astype(BF)
         gu_ref[deep, :] = total[128:256].T.astype(BF)
 
+    ring_step(7)
     for da in (1, 3, 2):
         q_copy(da).wait_recv()
 
@@ -329,6 +476,9 @@
     for da in range(3):
         whole = whole + qbuf[da, 0].astype(F32)
     town[...] = whole
+    exchanged(scanned, carried.at[rows_here], f_s.at[1], f_r.at[1])
+    carry_copy = rc(carried.at[rows_here], carried.at[rows_here], x_s.at[1], x_r.at[1], partner)
+    carry_copy.start()
     for db in (1, 3, 2):
         v_copy(db).wait_recv()
     whole = town[...]
@@ -354,25 +504,153 @@
     )
     take = take.astype(F32).astype(BF)
     own.wait()
+
+    distance = iota((LANES, LANES), 0) - iota((LANES, LANES), 1)
+    mask = jnp.where(
+        distance >= 0, jnp.exp(-rate * jnp.maximum(distance, 0).astype(F32)), 0.0
+    )
+    enter = jnp.exp(-rate * (steps + 1.0))
+    queries = q_ref[...]
+    rc(carried.at[rows_there], carried.at[rows_there], x_s.at[1], x_r.at[1], partner).wait_recv()
+
+    carry_copy.wait_send()
+
+    @pl.when(c == 1)
+    def _():
+        carried[...] = block_decay * carried[...] + state[0]
+
+    scores[...] = dot(queries, keys, 1, 1) * mask
+    retained = dot2(scores[...], vals) + enter * dot_2(queries, carried[...])
+    centered = retained - jnp.mean(retained, axis=-1, keepdims=True)
+    inv = lax.rsqrt(jnp.mean(centered * centered, axis=-1, keepdims=True) + NORM_EPS)
+    norm_s[...] = centered * inv
+    inv_s[...] = inv
+    mixes[c] = norm_s[...].astype(BF)
+    mix_copy = rc(mixes.at[c], mixes.at[c], x_s.at[2], x_r.at[2], partner)
+    mix_copy.start()
+    ring_step(8)
     for dz in range(1, nz):
         there = pl.ds(pl.multiple_of(lax.rem(z + nz - dz, nz) * BACK, 8), BACK)
         rc(rsend.at[here], ret.at[there], r_s.at[dz], r_r.at[dz], at_z(dz)).wait_recv()
-    mid_s[:, cols] = (cot_s[...].astype(F32) + dot(take, ret[...], 0, 0)).astype(BF)
+    mids[c, :, cols] = (cot_s[...].astype(F32) + dot(take, ret[...], 0, 0)).astype(BF)
 
     @pl.loop(1, 16)
     def _(k):
         dev = peer(k // 4, lax.rem(k, 4))
-        rc(mid_s.at[:, cols], mid_s.at[:, cols], m_s.at[k], m_r.at[k], dev).start()
+        rc(mids.at[c, :, cols], mids.at[c, :, cols], m_s.at[k], m_r.at[k], dev).start()
 
     @pl.loop(1, 16)
     def _(k):
         back = tid(lax.rem(4 - k // 4, 4), lax.rem(4 - lax.rem(k, 4), 4))
         theirs = pl.ds(pl.multiple_of(back * LANES, LANES), LANES)
         dev = peer(k // 4, lax.rem(k, 4))
-        rc(mid_s.at[:, cols], mid_s.at[:, theirs], m_s.at[k], m_r.at[k], dev).wait_recv()
-
-    mid_ref[...] = mid_s[...]
-
+        rc(mids.at[c, :, cols], mids.at[c, :, theirs], m_s.at[k], m_r.at[k], dev).wait_recv()
+
+    mid_copy = rc(mids.at[c], mids.at[c], x_s.at[3], x_r.at[3], partner)
+    mid_copy.start()
+    for dz in range(nz):
+        pass_on(dz, 1 - c).wait_recv()
+    head_grad = dot(mids[c], wfull[...])
+    normed = norm_s[...]
+    grad_ret = inv_s[...] * (
+        head_grad
+        - jnp.mean(head_grad, axis=-1, keepdims=True)
+        - normed * jnp.mean(head_grad * normed, axis=-1, keepdims=True)
+    )
+    start = jnp.exp(-rate * steps)
+    back_state[c] = dot_2(
+        queries, start * grad_ret, 0, 0
+    )
+    back_copy = rc(back_state.at[c], back_state.at[c], x_s.at[4], x_r.at[4], partner)
+    back_copy.start()
+
+    rc(mixes.at[1 - c], mixes.at[1 - c], x_s.at[2], x_r.at[2], partner).wait_recv()
+    rc(mids.at[1 - c], mids.at[1 - c], x_s.at[3], x_r.at[3], partner).wait_recv()
+
+    def partial_out(way, dz):
+        wide_cols = pl.ds(pl.multiple_of(lax.rem(z + dz, nz) * LANES, LANES), LANES)
+        prods[way] = dot(mids[0, :, wide_cols], mixes[0], 0, 0) + dot(
+            mids[1, :, wide_cols], mixes[1], 0, 0
+        )
+        return prods[way, pl.ds(pl.multiple_of(c * 64, 64), 64), :]
+
+    def up_copy(s):
+        return rc(up_s.at[s], up_r.at[s], o_s.at[0, s], o_r.at[0, s], at_z(1))
+
+    def dn_copy(s):
+        return rc(dn_s.at[s], dn_r.at[s], o_s.at[1, s], o_r.at[1, s], at_z(down))
+
+    def sum_step(s):
+        up = partial_out(0, far - s)
+        if s > 0:
+            up_copy(s - 1).wait_recv()
+            up = up + up_r[s - 1].astype(F32)
+        up_s[s] = up.astype(BF)
+        up_copy(s).start()
+        if s < far - 1:
+            dn = partial_out(1, nz - (far - 1 - s))
+            if s > 0:
+                dn_copy(s - 1).wait_recv()
+                dn = dn + dn_r[s - 1].astype(F32)
+            dn_s[s] = dn.astype(BF)
+            dn_copy(s).start()
+
+    sum_step(0)
+    rc(back_state.at[1 - c], back_state.at[1 - c], x_s.at[4], x_r.at[4], partner).wait_recv()
+    half_back[...] = (back_state[0, rows_here, :] + block_decay * back_state[1, rows_here, :]).astype(BF)
+    exchange(half_back, bslices, h_s.at[0], h_r.at[0])
+    sum_step(1)
+    score_grad = dot2(grad_ret, vals, 1, 1) * mask
+    grad_q = dot2(score_grad, keys)
+    high, low = split(grad_ret)
+    c_high, c_low = split(carried[...])
+    grad_q = grad_q + enter * (dot(high, c_high, 1, 1) + dot(low, c_high, 1, 1) + dot(high, c_low, 1, 1))
+    gq_ref[...] = grad_q.astype(BF)
+    sum_step(2)
+    exchanged(half_back, bslices, h_s.at[0], h_r.at[0])
+    running = jnp.zeros((8, 512), F32)
+    for e in range(nz - 1, -1, -1):
+        bscanned[e * 8 : e * 8 + 8, :] = running.astype(BF)
+        running = chip_decay * running + bslices[e * 8 : e * 8 + 8, :].astype(F32)
+    exchange(bscanned, future.at[rows_here], h_s.at[1], h_r.at[1])
+    sum_step(3)
+    score_t = scores[...]
+    s_high, s_low = split(score_t)
+    grad_v = dot(s_high, high, 0, 0) + dot(s_low, high, 0, 0) + dot(s_high, low, 0, 0)
+    grad_k = dot2(score_grad, queries, 0, 0)
+    sum_step(4)
+    exchanged(bscanned, future.at[rows_here], h_s.at[1], h_r.at[1])
+    future_copy = rc(future.at[rows_here], future.at[rows_here], x_s.at[5], x_r.at[5], partner)
+    future_copy.start()
+    sum_step(5)
+    rc(future.at[rows_there], future.at[rows_there], x_s.at[5], x_r.at[5], partner).wait_recv()
+    trail = jnp.exp(-rate * (LANES - steps))
+    ahead = future[...].astype(F32)
+    ahead = jnp.where(c == 0, back_state[1] + block_decay * ahead, ahead)
+    gv_ref[...] = (grad_v + trail * dot_2(keys, ahead)).astype(BF)
+    gk_ref[...] = ((grad_k + trail * dot_2(vals, ahead, 1, 1)) * scale).astype(BF)
+    sum_step(6)
+    sum_step(7)
+    total = partial_out(0, 0)
+    dn_copy(far - 2).wait_recv()
+    total = total + dn_r[far - 2].astype(F32)
+    up_copy(far - 1).wait_recv()
+    gow_ref[...] = total + up_r[far - 1].astype(F32)
+
+    for s in range(far):
+        up_copy(s).wait_send()
+        ring(0, s + 1).wait_send()
+        if s < far - 1:
+            dn_copy(s).wait_send()
+            ring(1, s + 1).wait_send()
+    for dz in range(nz):
+        pass_on(dz, c).wait_send()
+    exchange_sent(half_state, slices, f_s.at[0], f_r.at[0])
+    exchange_sent(scanned, carried.at[rows_here], f_s.at[1], f_r.at[1])
+    exchange_sent(half_back, bslices, h_s.at[0], h_r.at[0])
+    exchange_sent(bscanned, future.at[rows_here], h_s.at[1], h_r.at[1])
+    for copy in (state_copy, mix_copy, mid_copy, back_copy, future_copy):
+        copy.wait_send()
     for dz in range(1, nz):
         rc(sbuf.at[mine], xs.at[c, t, mine], z_s.at[dz], z_r.at[dz], at_z(dz)).wait_send()
         rc(rsend.at[here], ret.at[here], r_s.at[dz], r_r.at[dz], at_z(dz)).wait_send()
@@ -394,25 +672,45 @@
     @pl.loop(1, 16)
     def _(k):
         dev = peer(k // 4, lax.rem(k, 4))
-        rc(mid_s.at[:, cols], mid_s.at[:, cols], m_s.at[k], m_r.at[k], dev).wait_send()
-
-
-def moe(nz, routes, route_weights, cotangent, stream, gate, up, down):
+        rc(mids.at[c, :, cols], mids.at[c, :, cols], m_s.at[k], m_r.at[k], dev).wait_send()
+
+
+def local(
+    cotangent,
+    stream,
+    routes,
+    route_weights,
+    gate_proj,
+    up_proj,
+    down_proj,
+    out_weight,
+    queries,
+    keys,
+    values,
+    decay_rate,
+):
+    nz = lax.axis_size("z")
     width = cotangent.shape[1]
     rows, kept = nz * PAIR, nz * SLOTS
+    far = nz // 2
     any_ = pl.BlockSpec(memory_space=pl.ANY)
     vmem = pl.BlockSpec(memory_space=pltpu.VMEM)
     dma = pltpu.SemaphoreType.DMA
-    return pl.pallas_call(
-        functools.partial(moe_kernel, nz),
+    grads = pl.pallas_call(
+        functools.partial(kernel, nz),
         out_shape=(
             jax.ShapeDtypeStruct((width, LANES), BF),
             jax.ShapeDtypeStruct((width, LANES), BF),
             jax.ShapeDtypeStruct((LANES, width), BF),
-            jax.ShapeDtypeStruct((LANES, width), BF),
+            jax.ShapeDtypeStruct(out_weight.shape, F32),
+            jax.ShapeDtypeStruct(queries.shape, BF),
+            jax.ShapeDtypeStruct(keys.shape, BF),
+            jax.ShapeDtypeStruct(values.shape, BF),
         ),
-        in_specs=[vmem, vmem, any_, any_, any_, any_, any_],
-        out_specs=(vmem,) * 4,
+        in_specs=[vmem, vmem]
+        + [any_] * 6
+        + [vmem, vmem, vmem, pl.BlockSpec(memory_space=pltpu.SMEM)],
+        out_specs=(vmem,) * 7,
         scratch_shapes=[
             pltpu.VMEM((2, width, 2 * LANES), BF),
             pltpu.VMEM((LANES, width), BF),
@@ -434,8 +732,28 @@
             pltpu.VMEM((3, kept, LANES), BF),
             pltpu.VMEM((nz * BACK, LANES), BF),
             pltpu.VMEM((nz * BACK, LANES), BF),
-            pltpu.VMEM((LANES, width), BF),
-            dma((7,)),
+            pltpu.VMEM((2, LANES, width), BF),
+            pltpu.VMEM((width, 512), BF),
+            pltpu.VMEM((2, 256, 512), F32),
+            pltpu.VMEM((128, 512), F32),
+            pltpu.VMEM((128, 512), F32),
+            pltpu.VMEM((128, 512), F32),
+            pltpu.VMEM((256, 512), F32),
+            pltpu.VMEM((2, LANES, 512), BF),
+            pltpu.VMEM((LANES, LANES), F32),
+            pltpu.VMEM((LANES, 512), F32),
+            pltpu.VMEM((LANES, 1), F32),
+            pltpu.VMEM((2, 256, 512), F32),
+            pltpu.VMEM((128, 512), BF),
+            pltpu.VMEM((128, 512), BF),
+            pltpu.VMEM((128, 512), BF),
+            pltpu.VMEM((256, 512), BF),
+            pltpu.VMEM((2, LANES, 512), F32),
+            pltpu.VMEM((far, 64, 512), BF),
+            pltpu.VMEM((far, 64, 512), BF),
+            pltpu.VMEM((far - 1, 64, 512), BF),
+            pltpu.VMEM((far - 1, 64, 512), BF),
+            dma((8,)),
             dma((nz,)),
             dma((nz,)),
             dma,
@@ -456,97 +774,38 @@
             dma((nz,)),
             dma((16,)),
             dma((16,)),
+            dma((2, far + 1)),
+            dma((2, far + 1)),
+            dma((nz,)),
+            dma((nz,)),
+            dma((6,)),
+            dma((6,)),
+            dma((2, nz)),
+            dma((2, nz)),
+            dma((2, nz)),
+            dma((2, nz)),
+            dma((2, far)),
+            dma((2, far)),
         ],
         compiler_params=pltpu.CompilerParams(
-            collective_id=0, has_side_effects=True, vmem_limit_bytes=56 * 2**20
+            collective_id=0, has_side_effects=True, vmem_limit_bytes=58 * 2**20
         ),
-        cost_estimate=pl.CostEstimate(flops=60_000_000_000, bytes_accessed=0, transcendentals=0),
-        name="moe",
-    )(routes.T, route_weights, cotangent, stream, gate, up, down)
-
-
-def owner_scan(state, weights):
-    parts = weights.shape[0]
-    piece = state.astype(BF).reshape(parts, -1, state.shape[1])
-    piece = lax.all_to_all(piece, SP, 0, 0, tiled=True)
-    mixed = jnp.einsum(
-        "bj,jxy->bxy", weights, piece.astype(F32), precision=lax.Precision.HIGHEST
-    ).astype(BF)
-    return lax.all_to_all(mixed, SP, 0, 0, tiled=True).reshape(state.shape)
-
-
-def local(
-    cotangent,
-    stream,
-    routes,
-    route_weights,
-    gate_proj,
-    up_proj,
-    down_proj,
-    out_weight,
-    queries,
-    keys,
-    values,
-    decay_rate,
-):
-    nz = lax.axis_size("z")
-    blocks = 2 * nz
-    tok_rows = cotangent.shape[0]
-    rate = decay_rate[0]
-    steps = jnp.arange(tok_rows, dtype=F32)
-    distance = steps[:, None] - steps[None, :]
-    mask = jnp.where(distance >= 0, jnp.exp(-rate * jnp.maximum(distance, 0.0)), 0.0)
-    enter = jnp.exp(-rate * (steps + 1.0))[:, None]
-    leave = jnp.exp(-rate * (tok_rows - 1.0 - steps))[:, None]
-    start = jnp.exp(-rate * steps)[:, None]
-    trail = jnp.exp(-rate * (tok_rows - steps))[:, None]
-    order = jnp.arange(blocks, dtype=F32)
-    apart = order[:, None] - order[None, :] - 1.0
-    earlier = jnp.where(apart >= 0, jnp.exp(-rate * tok_rows * jnp.maximum(apart, 0.0)), 0.0)
-    later = earlier.T
-    keys = keys * BF(keys.shape[1] ** -0.5)
-    key_wide = keys.astype(F32)
-    query_wide = queries.astype(F32)
-    carried = owner_scan(dot((key_wide * leave).astype(BF), values, 0, 0), earlier)
-    scores = dot(queries, keys, 1, 1) * mask
-    scores_b = scores.astype(BF)
-    retained = dot(scores_b, values) + enter * dot(queries, carried)
-    centered = retained - jnp.mean(retained, axis=-1, keepdims=True)
-    inv_scale = lax.rsqrt(jnp.mean(centered * centered, axis=-1, keepdims=True) + NORM_EPS)
-    normed = centered * inv_scale
-    mixed = normed.astype(BF)
-    weight = lax.all_gather(out_weight, SP, axis=0, tiled=True)
-
-    grad_gate, grad_up, grad_down, mid_grad = moe(
-        nz, routes, route_weights, cotangent, stream, gate_proj[0], up_proj[0], down_proj[0]
+        name="layer_backward",
+    )(
+        routes.T,
+        route_weights,
+        cotangent,
+        stream,
+        gate_proj[0],
+        up_proj[0],
+        down_proj[0],
+        out_weight,
+        queries,
+        keys,
+        values,
+        decay_rate,
     )
-
-    head_grad = dot(mid_grad, weight)
-    grad_out_weight = dot(mid_grad, mixed, 0, 0)
-    for axis in SP:
-        grad_out_weight = lax.psum_scatter(grad_out_weight, axis, scatter_dimension=0, tiled=True)
-    grad_retained = inv_scale * (
-        head_grad
-        - jnp.mean(head_grad, axis=-1, keepdims=True)
-        - normed * jnp.mean(head_grad * normed, axis=-1, keepdims=True)
-    )
-    ret_b = grad_retained.astype(BF)
-    future = owner_scan(dot((query_wide * start).astype(BF), ret_b, 0, 0), later)
-    score_grad = (dot(ret_b, values, 1, 1) * mask).astype(BF)
-    grad_queries = dot(score_grad, keys) + enter * dot(ret_b, carried, 1, 1)
-    grad_keys = (
-        dot(score_grad, queries, 0, 0) + trail * dot(values, future, 1, 1)
-    ) * queries.shape[1] ** (-0.5)
-    grad_values = dot(scores_b, ret_b, 0, 0) + trail * dot(keys, future)
-    return (
-        grad_gate[None],
-        grad_up[None],
-        grad_down[None],
-        grad_out_weight,
-        grad_queries.astype(BF),
-        grad_keys.astype(BF),
-        grad_values.astype(BF),
-    )
+    return tuple(g[None] for g in grads[:3]) + tuple(grads[3:])
 
 
 def solution(mesh):

time: 288 us -> 160 us (0.56)
  waiting for transfers between devices: 115 us -> 0 us
  Pallas kernels: 103 us -> 148 us
  starting transfers between devices: 34.5 us -> 0 us
  between operations: 16.4 us -> 1.31 us
  matrix products: 12.5 us -> 0 us
    reduce_scatter x2 -> x0, waiting for transfers between devices: 69.5 us -> none  [local(): lax.psum_scatter(grad_out_weight, axis, scatter_dimension=0, tiled=True)]
    pallas_call x1, Pallas kernels: 103 us -> 148 us  [local(): pl.pallas_call(functools.partial(kernel, nz), out_shape=(jax.ShapeDtypeSt...]
    all_to_all x4 -> x0, waiting for transfers between devices: 45.2 us -> none  [the longest x2 45.2 us: owner_scan(): piece = lax.all_to_all(piece, SP, 0, 0, tiled=True)]
    all_to_all x4 -> x0, starting transfers between devices: 34.4 us -> none  [the longest x2 26 us: owner_scan(): piece = lax.all_to_all(piece, SP, 0, 0, tiled=True)]
    dot_general x16 -> x0, matrix products: 12.5 us -> none  [the longest x14 11.6 us: dot(): lax.dot_general(a, b, (((left,), (right,)), ((), ())), preferred_element_...]
    unnamed x18 -> x22, local copies, waits for them, and re-layouts: 4.16 us -> 8.37 us
  transfers between devices with their start and end apart: 7 -> 0, of which waited for: 4 -> 0; matrix products, arithmetic and copies ran while one was open for 5% -> 0% of each run, Pallas kernels for 36% -> 0%
where the time goes in v2:
time: 160 us; the launch traced here: 158 us
  Pallas kernels  148 us (92%)
  local copies, waits for them, and re-layouts  8.37 us (5%)
    pallas_call x1, Pallas kernels, local(): pl.pallas_call(functools.partial(kernel, nz), out_shape=(jax.ShapeDtypeSt...  148 us
    unnamed x22, local copies, waits for them, and re-layouts  8.37 us

profile of v2, /device:TPU:1, one launch (start us, length us, event | category | flops | bytes accessed | tf_op | source)
XLA Modules:
  0.0 157.9 jit_solution(14117599866537673687)
XLA Ops:
  1.3 0.0 copy-start.6
  1.3 0.7 copy-done.6
  2.0 0.7 copy.19.weights_ref
  2.7 148.2 %layer_backward.1 = (bf16[2048,128]{1,0:T(8,128)(2,1)}, bf16[2048,128]{1,0:T(8,128)(2,1)}, bf16[128,2048]{1,0:T(8,128)(2,1)}, f32[64,512]{1,0:T(8,128)}, bf16[12...) custom-call(s32[2,128]{1,0:T(2,128)} %bitcast.13, f32[128,2]{1,0:T(8,128)} %copy.19.weights_ref, ...), custom_call_target="tpu_custom_call" | custom-call | tf_op jit(solution)/shard_map/layer_backward/pallas_call | solution.py:699
  150.9 0.0 copy-start.1
  150.9 1.9 %copy.28 = bf16[1,2048,128]{2,1,0:T(8,128)(2,1)} copy(bf16[1,2048,128]{2,1,0:T(8,128)(2,1)} %bitcast.9) | data formatting | bytes 1048576
  152.9 0.0 copy-done.1
  152.9 0.0 copy-start
  152.9 0.8 copy.29
  153.7 0.4 copy-done
  154.1 0.0 copy-start.3
  154.1 0.8 copy.30
  154.9 0.2 copy-done.3
  155.1 0.0 copy-start.5
  155.1 0.0 copy-start.4
  155.1 0.7 copy.31
  155.8 0.2 copy-done.5
  156.0 0.0 copy-start.2
  156.0 0.6 copy.32
  156.6 0.0 copy-done.4
  156.6 0.6 copy.33
  157.3 0.0 copy-done.2
  157.3 0.7 copy.34
Async XLA Ops:
  1.3 0.7 copy-start.6
  150.9 1.9 %copy-start.1 = (bf16[2048,128]{1,0:T(8,128)(2,1)S(1)}, bf16[2048,128]{1,0:T(8,128)(2,1)}, u32[]{:S(2)}) copy-start(bf16[2048,128]{1,0:T(8,128)(2,1)} %get-tuple-element.15) | copy-start | bytes 1572868
  152.9 1.2 copy-start
  154.1 1.0 copy-start.3
  155.1 0.9 copy-start.5
  155.1 1.5 copy-start.4
  156.0 1.3 copy-start.2

commit v3 on v2

--- a/solution.py
+++ b/solution.py
@@ -82,15 +82,20 @@
     norm_s,
     inv_s,
     back_state,
-    half_back,
+    whole_back,
     bslices,
     bscanned,
     future,
-    prods,
     up_s,
     up_r,
     dn_s,
     dn_r,
+    part_v,
+    part_k,
+    ret_s,
+    sgrad,
+    gow_s,
+    entered,
     loc,
     z_s,
     z_r,
@@ -285,19 +290,22 @@
         here = pl.ds(pl.multiple_of(lax.rem(z + nz - dz, nz) * PAIR, 8), PAIR)
         rc(sbuf.at[mine], xs.at[c, t, here], z_s.at[dz], z_r.at[dz], at_z(dz)).wait_recv()
 
-    def product(core, piece):
-        a = xs[core, piece]
-        deep = pl.ds(pl.multiple_of(piece * LANES, LANES), LANES)
-        acc[core, :, 0:256] += dot(a, wcat[0, deep, :])
-        acc[core, :, 256:384] += dot(a, down_v[:, deep], 1, 1)
+    def product(core, pieces):
+        deep = [pl.ds(pl.multiple_of(piece * LANES, LANES), LANES) for piece in pieces]
+        a = jnp.concatenate([xs[core, piece] for piece in pieces], axis=1)
+        acc[core, :, 0:256] += dot(a, jnp.concatenate([wcat[0, d, :] for d in deep], axis=0))
+        acc[core, :, 256:384] += dot(a, jnp.concatenate([down_v[:, d] for d in deep], axis=1), 1, 1)
 
     first = pl.ds(0, half)
     last = pl.ds(half, half)
 
-    def a_copy(k, piece):
-        part = (slice(None), slice(None), first, last)[k]
-        ref = xs.at[c, piece] if k < 2 else xs.at[c, piece, part]
-        return rc(ref, ref, a_s.at[k], a_r.at[k], peer(1 if k % 2 == 0 else 3, 0))
+    def a_copy(da):
+        ref = xs.at[c, t]
+        return rc(ref, ref, a_s.at[da], a_r.at[da], peer(da, 0))
+
+    def a_got(da):
+        ref = xs.at[c, tid(4 - da, 0)]
+        rc(ref, ref, a_s.at[da], a_r.at[da], peer(da, 0)).wait_recv()
 
     def b_copy(i, k, piece):
         part = (slice(None), slice(None), first, last)[k]
@@ -313,81 +321,81 @@
         b_copy(i, 1, piece).start()
         d_copy(i, 0, c, piece).start()
 
-    a_copy(0, t).start()
-    a_copy(1, t).start()
+    for da in (1, 3, 2):
+        a_copy(da).start()
     spread(0, t)
-    product(c, t)
-    piece = tid(3, 0)
-    a_copy(0, piece).wait_recv()
-    a_copy(2, piece).start()
-    spread(1, piece)
-    other = tid(1, 0)
-    a_copy(1, other).wait_recv()
-    a_copy(3, other).start()
-    spread(2, other)
-    product(c, piece)
-    product(c, other)
-    piece = tid(2, 0)
-    a_copy(2, piece).wait_recv()
-    a_copy(3, piece).wait_recv()
-    spread(3, piece)
-    product(c, piece)
+    ring_step(1)
+    for i, da in ((1, 1), (2, 3), (3, 2)):
+        a_got(da)
+        spread(i, tid(4 - da, 0))
+    ring_step(2)
 
     rows_here = pl.ds(pl.multiple_of(c * 128, 128), 128)
     rows_there = pl.ds(pl.multiple_of((1 - c) * 128, 128), 128)
 
-    def slice_of(dz):
-        return pl.ds(pl.multiple_of(lax.rem(z + dz, nz) * 8, 8), 8)
-
-    def exchange(src, dst, ss, rs):
+    def slice_of(dz, n):
+        return pl.ds(pl.multiple_of(lax.rem(z + dz, nz) * n, 8), n)
+
+    def exchange(src, dst, ss, rs, n=8):
         for k in range(1, nz):
             dz = nz // 2 + (k // 2 if k % 2 == 0 else -(k // 2))
-            rc(src.at[slice_of(dz)], dst.at[slice_of(0)], ss.at[dz], rs.at[dz], at_z(dz)).start()
-        mine_copy = pltpu.make_async_copy(src.at[slice_of(0)], dst.at[slice_of(0)], ss.at[0])
+            rc(src.at[slice_of(dz, n)], dst.at[slice_of(0, n)], ss.at[dz], rs.at[dz], at_z(dz)).start()
+        mine_copy = pltpu.make_async_copy(src.at[slice_of(0, n)], dst.at[slice_of(0, n)], ss.at[0])
         mine_copy.start()
 
-    def exchanged(src, dst, ss, rs):
-        pltpu.make_async_copy(src.at[slice_of(0)], dst.at[slice_of(0)], ss.at[0]).wait()
+    def exchanged(src, dst, ss, rs, n=8):
+        pltpu.make_async_copy(src.at[slice_of(0, n)], dst.at[slice_of(0, n)], ss.at[0]).wait()
         for dz in range(1, nz):
             rc(
-                src.at[slice_of(0)], dst.at[slice_of(nz - dz)], ss.at[dz], rs.at[dz], at_z(dz)
+                src.at[slice_of(0, n)], dst.at[slice_of(nz - dz, n)], ss.at[dz], rs.at[dz], at_z(dz)
             ).wait_recv()
 
-    def exchange_sent(src, dst, ss, rs):
+    def exchange_sent(src, dst, ss, rs, n=8):
         for dz in range(1, nz):
-            rc(src.at[slice_of(0)], dst.at[slice_of(0)], ss.at[dz], rs.at[dz], at_z(dz)).wait_send()
+            rc(src.at[slice_of(0, n)], dst.at[slice_of(0, n)], ss.at[dz], rs.at[dz], at_z(dz)).wait_send()
 
     rc(state.at[1 - c], state.at[1 - c], x_s.at[0], x_r.at[0], partner).wait_recv()
     half_state[...] = block_decay * state[0, rows_here, :] + state[1, rows_here, :]
-    exchange(half_state, slices, f_s.at[0], f_r.at[0])
 
     def offset(i):
         return (lax.rem(i + 1, 3) + 1) * jnp.minimum(i, 1)
+
+    def theirs_in(i):
+        da = offset(i)
+        pieces = [other_tid(da, db) for db in (0, 3, 1, 2)]
+        for j in range(4):
+            d_copy(i, j, 1 - c, pieces[j]).wait_recv()
+        product(1 - c, pieces)
 
     @pl.loop(0, 4)
     def _(i):
         da = offset(i)
-        left, right, far = tid(da, 3), tid(da, 1), tid(da, 2)
+        left, right, far_piece = tid(da, 3), tid(da, 1), tid(da, 2)
         b_copy(i, 0, left).wait_recv()
         b_copy(i, 2, left).start()
         d_copy(i, 1, c, left).start()
         b_copy(i, 1, right).wait_recv()
         b_copy(i, 3, right).start()
         d_copy(i, 2, c, right).start()
-        product(c, left)
-        product(c, right)
-        b_copy(i, 2, far).wait_recv()
-        b_copy(i, 3, far).wait_recv()
-        d_copy(i, 3, c, far).start()
-        product(c, far)
-        for j in range(4):
-            piece = other_tid(da, (0, 3, 1, 2)[j])
-            d_copy(i, j, 1 - c, piece).wait_recv()
-            product(1 - c, piece)
-        for s in range(1, 5):
-            @pl.when(i == s - 1)
+
+        @pl.when(i > 0)
+        def _():
+            theirs_in(i - 1)
+
+        b_copy(i, 2, far_piece).wait_recv()
+        b_copy(i, 3, far_piece).wait_recv()
+        d_copy(i, 3, c, far_piece).start()
+        product(c, [tid(da, 0), left, right, far_piece])
+
+        for s in range(3):
+
+            @pl.when(i == s)
             def _():
-                ring_step(s)
+                ring_step(3 + s)
+
+    theirs_in(3)
+    ring_step(6)
+    exchange(half_state, slices, f_s.at[0], f_r.at[0])
 
     @pl.loop(0, 2 * rows // 80)
     def _(k):
@@ -409,14 +417,6 @@
         wide[core, at, 128:256] = jnp.where(is_in, grad_up, 0.0).astype(BF)
         wide[core, at, 256:384] = jnp.where(is_in, 0.0, pltpu.roll(hidden, 60, axis=0)).astype(BF)
 
-    exchanged(half_state, slices, f_s.at[0], f_r.at[0])
-    running = jnp.zeros((8, 512), F32)
-    for e in range(nz):
-        scanned[e * 8 : e * 8 + 8, :] = running
-        running = chip_decay * running + slices[e * 8 : e * 8 + 8, :]
-    exchange(scanned, carried.at[rows_here], f_s.at[1], f_r.at[1])
-    ring_step(5)
-
     low = iota((kept, rows), 0)
     pick = (iota((kept, rows), 1) == low + SLOTS * ((low * 3277) // 65536) + SLOTS)
     pick = pick.astype(F32).astype(BF)
@@ -427,38 +427,55 @@
     weight_copy.wait_recv()
     grad_copy.wait_recv()
 
-    def partial_in(piece):
-        deep = pl.ds(pl.multiple_of(piece * LANES, LANES), LANES)
-        return dot(gown[...], wcat[0, deep, :], 1, 1) + dot(gpart[...], wcat[1, deep, :], 1, 1)
+    def partial_in(pieces):
+        deep = [pl.ds(pl.multiple_of(piece * LANES, LANES), LANES) for piece in pieces]
+        own_w, their_w = (jnp.concatenate([wcat[k, d, :] for d in deep], axis=0) for k in range(2))
+        return dot(gown[...], own_w, 1, 1) + dot(gpart[...], their_w, 1, 1)
 
     def q_copy(da):
         return rc(pbuf.at[da - 1], qbuf.at[da - 1], q_s.at[da - 1], q_r.at[da - 1], peer(da, 0))
 
     for da in (2, 1, 3):
 
-        @pl.loop(0, 4)
-        def _(db):
-            pbuf[da - 1, db] = partial_in(tid(da, db)).astype(BF)
+        for db in (0, 2):
+            both = partial_in((tid(da, db), tid(da, db + 1))).astype(BF)
+            pbuf[da - 1, db] = both[:, 0:LANES]
+            pbuf[da - 1, db + 1] = both[:, LANES:]
 
         q_copy(da).start()
 
-    @pl.loop(0, 4)
-    def _(db):
-        pown[db] = partial_in(tid(0, db))
-
-    ring_step(6)
+    for db in (0, 2):
+        both = partial_in((tid(0, db), tid(0, db + 1)))
+        pown[db] = both[:, 0:LANES]
+        pown[db + 1] = both[:, LANES:]
 
     for core in range(2):
         wide_t[core] = wide[core].T
 
-    @pl.loop(0, 16)
-    def _(piece):
-        deep = pl.ds(pl.multiple_of(piece * LANES, LANES), LANES)
-        total = dot(wide_t[0], xs[0, piece]) + dot(wide_t[1], xs[1, piece])
+    def weight_grads(pair):
+        deep = pl.ds(pl.multiple_of(pair * 2 * LANES, 2 * LANES), 2 * LANES)
+        total = 0.0
+        for core in range(2):
+            both = jnp.concatenate([xs[core, pair * 2], xs[core, pair * 2 + 1]], axis=1)
+            total = total + dot(wide_t[core], both)
         gd_ref[:, deep] = total[256:384].astype(BF)
         gg_ref[deep, :] = total[0:128].T.astype(BF)
         gu_ref[deep, :] = total[128:256].T.astype(BF)
 
+    @pl.loop(0, 4)
+    def _(pair):
+        weight_grads(pair)
+
+    @pl.loop(4, 8)
+    def _(pair):
+        weight_grads(pair)
+
+    exchanged(half_state, slices, f_s.at[0], f_r.at[0])
+    running = jnp.zeros((8, 512), F32)
+    for e in range(nz):
+        scanned[e * 8 : e * 8 + 8, :] = running.astype(BF)
+        running = chip_decay * running + slices[e * 8 : e * 8 + 8, :]
+    exchange(scanned, entered.at[rows_here], f_s.at[1], f_r.at[1])
     ring_step(7)
     for da in (1, 3, 2):
         q_copy(da).wait_recv()
@@ -476,9 +493,6 @@
     for da in range(3):
         whole = whole + qbuf[da, 0].astype(F32)
     town[...] = whole
-    exchanged(scanned, carried.at[rows_here], f_s.at[1], f_r.at[1])
-    carry_copy = rc(carried.at[rows_here], carried.at[rows_here], x_s.at[1], x_r.at[1], partner)
-    carry_copy.start()
     for db in (1, 3, 2):
         v_copy(db).wait_recv()
     whole = town[...]
@@ -504,6 +518,9 @@
     )
     take = take.astype(F32).astype(BF)
     own.wait()
+    exchanged(scanned, entered.at[rows_here], f_s.at[1], f_r.at[1])
+    carry_copy = rc(entered.at[rows_here], entered.at[rows_here], x_s.at[1], x_r.at[1], partner)
+    carry_copy.start()
 
     distance = iota((LANES, LANES), 0) - iota((LANES, LANES), 1)
     mask = jnp.where(
@@ -511,14 +528,10 @@
     )
     enter = jnp.exp(-rate * (steps + 1.0))
     queries = q_ref[...]
-    rc(carried.at[rows_there], carried.at[rows_there], x_s.at[1], x_r.at[1], partner).wait_recv()
-
-    carry_copy.wait_send()
-
-    @pl.when(c == 1)
-    def _():
-        carried[...] = block_decay * carried[...] + state[0]
-
+    rc(entered.at[rows_there], entered.at[rows_there], x_s.at[1], x_r.at[1], partner).wait_recv()
+
+    inside = entered[...].astype(F32)
+    carried[...] = jnp.where(c == 1, block_decay * inside + state[0], inside)
     scores[...] = dot(queries, keys, 1, 1) * mask
     retained = dot2(scores[...], vals) + enter * dot_2(queries, carried[...])
     centered = retained - jnp.mean(retained, axis=-1, keepdims=True)
@@ -527,7 +540,11 @@
     inv_s[...] = inv
     mixes[c] = norm_s[...].astype(BF)
     mix_copy = rc(mixes.at[c], mixes.at[c], x_s.at[2], x_r.at[2], partner)
-    mix_copy.start()
+
+    @pl.when(c == 0)
+    def _():
+        mix_copy.start()
+
     ring_step(8)
     for dz in range(1, nz):
         there = pl.ds(pl.multiple_of(lax.rem(z + nz - dz, nz) * BACK, 8), BACK)
@@ -547,7 +564,11 @@
         rc(mids.at[c, :, cols], mids.at[c, :, theirs], m_s.at[k], m_r.at[k], dev).wait_recv()
 
     mid_copy = rc(mids.at[c], mids.at[c], x_s.at[3], x_r.at[3], partner)
-    mid_copy.start()
+
+    @pl.when(c == 0)
+    def _():
+        mid_copy.start()
+
     for dz in range(nz):
         pass_on(dz, 1 - c).wait_recv()
     head_grad = dot(mids[c], wfull[...])
@@ -562,102 +583,140 @@
         queries, start * grad_ret, 0, 0
     )
     back_copy = rc(back_state.at[c], back_state.at[c], x_s.at[4], x_r.at[4], partner)
-    back_copy.start()
-
-    rc(mixes.at[1 - c], mixes.at[1 - c], x_s.at[2], x_r.at[2], partner).wait_recv()
-    rc(mids.at[1 - c], mids.at[1 - c], x_s.at[3], x_r.at[3], partner).wait_recv()
-
-    def partial_out(way, dz):
+    ret_s[...] = grad_ret
+
+    def partial_out(dz):
         wide_cols = pl.ds(pl.multiple_of(lax.rem(z + dz, nz) * LANES, LANES), LANES)
-        prods[way] = dot(mids[0, :, wide_cols], mixes[0], 0, 0) + dot(
+        return dot(mids[0, :, wide_cols], mixes[0], 0, 0) + dot(
             mids[1, :, wide_cols], mixes[1], 0, 0
         )
-        return prods[way, pl.ds(pl.multiple_of(c * 64, 64), 64), :]
-
-    def up_copy(s):
-        return rc(up_s.at[s], up_r.at[s], o_s.at[0, s], o_r.at[0, s], at_z(1))
-
-    def dn_copy(s):
-        return rc(dn_s.at[s], dn_r.at[s], o_s.at[1, s], o_r.at[1, s], at_z(down))
+
+    def up_copy(s, side):
+        at = (s, pl.ds(side * 32, 32))
+        return rc(up_s.at[at], up_r.at[at], o_s.at[0, s, side], o_r.at[0, s, side], at_z(1))
+
+    def dn_copy(s, side):
+        at = (s, pl.ds(side * 32, 32))
+        return rc(dn_s.at[at], dn_r.at[at], o_s.at[1, s, side], o_r.at[1, s, side], at_z(down))
 
     def sum_step(s):
-        up = partial_out(0, far - s)
-        if s > 0:
-            up_copy(s - 1).wait_recv()
-            up = up + up_r[s - 1].astype(F32)
-        up_s[s] = up.astype(BF)
-        up_copy(s).start()
+        up = partial_out(far - s)
         if s < far - 1:
-            dn = partial_out(1, nz - (far - 1 - s))
+            dn = partial_out(nz - (far - 1 - s))
+        for side in range(4):
+            part = slice(side * 32, side * 32 + 32)
+            whole = up[part]
             if s > 0:
-                dn_copy(s - 1).wait_recv()
-                dn = dn + dn_r[s - 1].astype(F32)
-            dn_s[s] = dn.astype(BF)
-            dn_copy(s).start()
-
-    sum_step(0)
-    rc(back_state.at[1 - c], back_state.at[1 - c], x_s.at[4], x_r.at[4], partner).wait_recv()
-    half_back[...] = (back_state[0, rows_here, :] + block_decay * back_state[1, rows_here, :]).astype(BF)
-    exchange(half_back, bslices, h_s.at[0], h_r.at[0])
-    sum_step(1)
-    score_grad = dot2(grad_ret, vals, 1, 1) * mask
-    grad_q = dot2(score_grad, keys)
-    high, low = split(grad_ret)
-    c_high, c_low = split(carried[...])
-    grad_q = grad_q + enter * (dot(high, c_high, 1, 1) + dot(low, c_high, 1, 1) + dot(high, c_low, 1, 1))
-    gq_ref[...] = grad_q.astype(BF)
-    sum_step(2)
-    exchanged(half_back, bslices, h_s.at[0], h_r.at[0])
-    running = jnp.zeros((8, 512), F32)
-    for e in range(nz - 1, -1, -1):
-        bscanned[e * 8 : e * 8 + 8, :] = running.astype(BF)
-        running = chip_decay * running + bslices[e * 8 : e * 8 + 8, :].astype(F32)
-    exchange(bscanned, future.at[rows_here], h_s.at[1], h_r.at[1])
-    sum_step(3)
-    score_t = scores[...]
-    s_high, s_low = split(score_t)
-    grad_v = dot(s_high, high, 0, 0) + dot(s_low, high, 0, 0) + dot(s_high, low, 0, 0)
-    grad_k = dot2(score_grad, queries, 0, 0)
-    sum_step(4)
-    exchanged(bscanned, future.at[rows_here], h_s.at[1], h_r.at[1])
-    future_copy = rc(future.at[rows_here], future.at[rows_here], x_s.at[5], x_r.at[5], partner)
-    future_copy.start()
-    sum_step(5)
-    rc(future.at[rows_there], future.at[rows_there], x_s.at[5], x_r.at[5], partner).wait_recv()
+                up_copy(s - 1, side).wait_recv()
+                whole = whole + up_r[s - 1, part, :].astype(F32)
+            up_s[s, part, :] = whole.astype(BF)
+            up_copy(s, side).start()
+            if s < far - 1:
+                whole = dn[part]
+                if s > 0:
+                    dn_copy(s - 1, side).wait_recv()
+                    whole = whole + dn_r[s - 1, part, :].astype(F32)
+                dn_s[s, part, :] = whole.astype(BF)
+                dn_copy(s, side).start()
+
+    def query_part():
+        grad = ret_s[...]
+        high, low = split(grad)
+        sgrad[...] = dot2(grad, vals, 1, 1) * mask
+        c_high, c_low = split(carried[...])
+        carry = dot(high, c_high, 1, 1) + dot(low, c_high, 1, 1) + dot(high, c_low, 1, 1)
+        gq_ref[...] = (dot2(sgrad[...], keys) + enter * carry).astype(BF)
+
+    def value_part():
+        high, low = split(ret_s[...])
+        s_high, s_low = split(scores[...])
+        part_v[...] = dot(s_high, high, 0, 0) + dot(s_low, high, 0, 0) + dot(s_high, low, 0, 0)
+        part_k[...] = dot2(sgrad[...], queries, 0, 0)
+
+    future_copy = rc(future, future, x_s.at[5], x_r.at[5], partner)
+    gow_copy = rc(gow_s, gow_s, x_s.at[6], x_r.at[6], partner)
     trail = jnp.exp(-rate * (LANES - steps))
-    ahead = future[...].astype(F32)
-    ahead = jnp.where(c == 0, back_state[1] + block_decay * ahead, ahead)
-    gv_ref[...] = (grad_v + trail * dot_2(keys, ahead)).astype(BF)
-    gk_ref[...] = ((grad_k + trail * dot_2(vals, ahead, 1, 1)) * scale).astype(BF)
-    sum_step(6)
-    sum_step(7)
-    total = partial_out(0, 0)
-    dn_copy(far - 2).wait_recv()
-    total = total + dn_r[far - 2].astype(F32)
-    up_copy(far - 1).wait_recv()
-    gow_ref[...] = total + up_r[far - 1].astype(F32)
+
+    def last_products(ahead):
+        gv_ref[...] = (part_v[...] + trail * dot_2(keys, ahead)).astype(BF)
+        gk_ref[...] = ((part_k[...] + trail * dot_2(vals, ahead, 1, 1)) * scale).astype(BF)
+
+    @pl.when(c == 1)
+    def _():
+        back_copy.start()
+        rc(mixes.at[0], mixes.at[0], x_s.at[2], x_r.at[2], partner).wait_recv()
+        rc(mids.at[0], mids.at[0], x_s.at[3], x_r.at[3], partner).wait_recv()
+        sum_step(0)
+        query_part()
+        sum_step(1)
+        value_part()
+        for s in range(2, far):
+            sum_step(s)
+        total = partial_out(0)
+        for side in range(4):
+            part = slice(side * 32, side * 32 + 32)
+            dn_copy(far - 2, side).wait_recv()
+            up_copy(far - 1, side).wait_recv()
+            whole = (
+                total[part] + dn_r[far - 2, part, :].astype(F32) + up_r[far - 1, part, :].astype(F32)
+            )
+            if side < 2:
+                gow_s[part, :] = whole
+            else:
+                gow_ref[side * 32 - 64 : side * 32 - 32, :] = whole
+            if side == 1:
+                gow_copy.start()
+        future_copy.wait_recv()
+        last_products(future[...].astype(F32))
+        for s in range(far):
+            for side in range(4):
+                up_copy(s, side).wait_send()
+                if s < far - 1:
+                    dn_copy(s, side).wait_send()
+        back_copy.wait_send()
+        gow_copy.wait_send()
+
+    @pl.when(c == 0)
+    def _():
+        rc(back_state.at[1], back_state.at[1], x_s.at[4], x_r.at[4], partner).wait_recv()
+        whole_back[...] = (back_state[0] + block_decay * back_state[1]).astype(BF)
+        exchange(whole_back, bslices, h_s.at[0], h_r.at[0], 16)
+        query_part()
+        exchanged(whole_back, bslices, h_s.at[0], h_r.at[0], 16)
+        running = jnp.zeros((16, 512), F32)
+        for e in range(nz - 1, -1, -1):
+            bscanned[e * 16 : e * 16 + 16, :] = running.astype(BF)
+            running = chip_decay * running + bslices[e * 16 : e * 16 + 16, :].astype(F32)
+        exchange(bscanned, future, h_s.at[1], h_r.at[1], 16)
+        value_part()
+        exchanged(bscanned, future, h_s.at[1], h_r.at[1], 16)
+        future_copy.start()
+        last_products(back_state[1] + block_decay * future[...].astype(F32))
+        gow_copy.wait_recv()
+        gow_ref[...] = gow_s[...]
+        exchange_sent(whole_back, bslices, h_s.at[0], h_r.at[0], 16)
+        exchange_sent(bscanned, future, h_s.at[1], h_r.at[1], 16)
+        mix_copy.wait_send()
+        mid_copy.wait_send()
+        future_copy.wait_send()
 
     for s in range(far):
-        up_copy(s).wait_send()
         ring(0, s + 1).wait_send()
         if s < far - 1:
-            dn_copy(s).wait_send()
             ring(1, s + 1).wait_send()
     for dz in range(nz):
         pass_on(dz, c).wait_send()
     exchange_sent(half_state, slices, f_s.at[0], f_r.at[0])
-    exchange_sent(scanned, carried.at[rows_here], f_s.at[1], f_r.at[1])
-    exchange_sent(half_back, bslices, h_s.at[0], h_r.at[0])
-    exchange_sent(bscanned, future.at[rows_here], h_s.at[1], h_r.at[1])
-    for copy in (state_copy, mix_copy, mid_copy, back_copy, future_copy):
-        copy.wait_send()
+    exchange_sent(scanned, entered.at[rows_here], f_s.at[1], f_r.at[1])
+    state_copy.wait_send()
+    carry_copy.wait_send()
     for dz in range(1, nz):
         rc(sbuf.at[mine], xs.at[c, t, mine], z_s.at[dz], z_r.at[dz], at_z(dz)).wait_send()
         rc(rsend.at[here], ret.at[here], r_s.at[dz], r_r.at[dz], at_z(dz)).wait_send()
     weight_copy.wait_send()
     grad_copy.wait_send()
-    for k in range(4):
-        a_copy(k, t).wait_send()
+    for da in range(1, 4):
+        a_copy(da).wait_send()
 
     @pl.loop(0, 4)
     def _(i):
@@ -696,17 +755,18 @@
     any_ = pl.BlockSpec(memory_space=pl.ANY)
     vmem = pl.BlockSpec(memory_space=pltpu.VMEM)
     dma = pltpu.SemaphoreType.DMA
+    shapes = (
+        jax.ShapeDtypeStruct((width, LANES), BF),
+        jax.ShapeDtypeStruct((width, LANES), BF),
+        jax.ShapeDtypeStruct((LANES, width), BF),
+        jax.ShapeDtypeStruct(out_weight.shape, F32),
+        jax.ShapeDtypeStruct(queries.shape, BF),
+        jax.ShapeDtypeStruct(keys.shape, BF),
+        jax.ShapeDtypeStruct(values.shape, BF),
+    )
     grads = pl.pallas_call(
         functools.partial(kernel, nz),
-        out_shape=(
-            jax.ShapeDtypeStruct((width, LANES), BF),
-            jax.ShapeDtypeStruct((width, LANES), BF),
-            jax.ShapeDtypeStruct((LANES, width), BF),
-            jax.ShapeDtypeStruct(out_weight.shape, F32),
-            jax.ShapeDtypeStruct(queries.shape, BF),
-            jax.ShapeDtypeStruct(keys.shape, BF),
-            jax.ShapeDtypeStruct(values.shape, BF),
-        ),
+        out_shape=tuple(pltpu.VMEM(a.shape, a.dtype) for a in shapes),
         in_specs=[vmem, vmem]
         + [any_] * 6
         + [vmem, vmem, vmem, pl.BlockSpec(memory_space=pltpu.SMEM)],
@@ -737,22 +797,27 @@
             pltpu.VMEM((2, 256, 512), F32),
             pltpu.VMEM((128, 512), F32),
             pltpu.VMEM((128, 512), F32),
-            pltpu.VMEM((128, 512), F32),
+            pltpu.VMEM((128, 512), BF),
             pltpu.VMEM((256, 512), F32),
             pltpu.VMEM((2, LANES, 512), BF),
             pltpu.VMEM((LANES, LANES), F32),
             pltpu.VMEM((LANES, 512), F32),
             pltpu.VMEM((LANES, 1), F32),
             pltpu.VMEM((2, 256, 512), F32),
-            pltpu.VMEM((128, 512), BF),
-            pltpu.VMEM((128, 512), BF),
-            pltpu.VMEM((128, 512), BF),
             pltpu.VMEM((256, 512), BF),
-            pltpu.VMEM((2, LANES, 512), F32),
-            pltpu.VMEM((far, 64, 512), BF),
-            pltpu.VMEM((far, 64, 512), BF),
-            pltpu.VMEM((far - 1, 64, 512), BF),
-            pltpu.VMEM((far - 1, 64, 512), BF),
+            pltpu.VMEM((256, 512), BF),
+            pltpu.VMEM((256, 512), BF),
+            pltpu.VMEM((256, 512), BF),
+            pltpu.VMEM((far, LANES, 512), BF),
+            pltpu.VMEM((far, LANES, 512), BF),
+            pltpu.VMEM((far - 1, LANES, 512), BF),
+            pltpu.VMEM((far - 1, LANES, 512), BF),
+            pltpu.VMEM((LANES, 512), F32),
+            pltpu.VMEM((LANES, 256), F32),
+            pltpu.VMEM((LANES, 512), F32),
+            pltpu.VMEM((LANES, LANES), F32),
+            pltpu.VMEM((64, 512), F32),
+            pltpu.VMEM((256, 512), BF),
             dma((8,)),
             dma((nz,)),
             dma((nz,)),
@@ -778,14 +843,14 @@
             dma((2, far + 1)),
             dma((nz,)),
             dma((nz,)),
-            dma((6,)),
-            dma((6,)),
+            dma((7,)),
+            dma((7,)),
             dma((2, nz)),
             dma((2, nz)),
             dma((2, nz)),
             dma((2, nz)),
-            dma((2, far)),
-            dma((2, far)),
+            dma((2, far, 4)),
+            dma((2, far, 4)),
         ],
         compiler_params=pltpu.CompilerParams(
             collective_id=0, has_side_effects=True, vmem_limit_bytes=58 * 2**20

time: 160 us -> 145 us (0.906); the launches traced: 158 us -> 145 us
  Pallas kernels: 148 us -> 137 us
  local copies, waits for them, and re-layouts: 8.37 us -> 6.36 us
    pallas_call x1, Pallas kernels: 148 us -> 137 us  [local(): pl.pallas_call(functools.partial(kernel, nz), out_shape=tuple((pltpu.VMEM...]
    unnamed x22 -> x10, local copies, waits for them, and re-layouts: 8.37 us -> 6.36 us
where the time goes in v3:
time: 145 us
  Pallas kernels  137 us (94%)
  local copies, waits for them, and re-layouts  6.36 us (4%)
    pallas_call x1, Pallas kernels, local(): pl.pallas_call(functools.partial(kernel, nz), out_shape=tuple((pltpu.VMEM...  137 us
    unnamed x10, local copies, waits for them, and re-layouts  6.36 us

profile of v3, /device:TPU:1, one launch (start us, length us, event | category | flops | bytes accessed | tf_op | source)
XLA Modules:
  0.0 144.7 jit_solution(4569642893592380117)
XLA Ops:
  1.3 0.0 copy-start
  1.3 0.7 copy-done
  2.0 0.7 copy.19.weights_ref
  2.7 137.1 %layer_backward.1 = (bf16[2048,128]{1,0:T(8,128)(2,1)S(1)}, bf16[2048,128]{1,0:T(8,128)(2,1)S(1)}, bf16[128,2048]{1,0:T(8,128)(2,1)S(1)}, f32[64,512]{1,0:T(8,12...) custom-call(s32[2,128]{1,0:T(2,128)} %bitcast.13, ...), custom_call_target="tpu_custom_call" | custom-call | tf_op jit(solution)/shard_map/layer_backward/pallas_call | solution.py:767
  139.8 0.8 copy.27
  140.6 0.8 copy.28
  141.4 0.6 copy.31
  142.0 0.6 copy.32
  142.6 0.7 copy.30
  143.3 0.7 copy.33
  143.9 0.8 copy.29
Async XLA Ops:
  1.3 0.7 copy-start

commit v4 on v3

--- a/solution.py
+++ b/solution.py
@@ -239,8 +239,14 @@
         jnp.logical_or(places == slot[0] + SLOTS, places == slot[1] + SLOTS).astype(F32).astype(BF),
         str_s[...],
     )
+    same = (iota((LANES, LANES), 0) == iota((LANES, LANES), 1)).astype(F32).astype(BF)
+    top = weights_ref[...].astype(BF)
+    rest = weights_ref[...] - top.astype(F32)
+    mid = rest.astype(BF)
+    low = (rest - mid.astype(F32)).astype(BF)
+    columns = dot(same, top, 1, 1) + dot(same, mid, 1, 1) + dot(same, low, 1, 1)
     for k in range(2):
-        scaled = (weights_ref[:, k : k + 1] * cot).astype(BF)
+        scaled = (columns[:, k : k + 1] * cot).astype(BF)
         packed = packed + dot((places == slot[k]).astype(F32).astype(BF), scaled)
     sbuf[...] = packed.astype(BF)
 
@@ -355,46 +361,47 @@
             rc(src.at[slice_of(0, n)], dst.at[slice_of(0, n)], ss.at[dz], rs.at[dz], at_z(dz)).wait_send()
 
     rc(state.at[1 - c], state.at[1 - c], x_s.at[0], x_r.at[0], partner).wait_recv()
-    half_state[...] = block_decay * state[0, rows_here, :] + state[1, rows_here, :]
+    half_state[...] = (block_decay * state[0, rows_here, :] + state[1, rows_here, :]).astype(BF)
 
     def offset(i):
         return (lax.rem(i + 1, 3) + 1) * jnp.minimum(i, 1)
 
-    def theirs_in(i):
+    def near_from_partner(i):
         da = offset(i)
-        pieces = [other_tid(da, db) for db in (0, 3, 1, 2)]
-        for j in range(4):
+        pieces = [other_tid(da, db) for db in (0, 3, 1)]
+        for j in range(3):
             d_copy(i, j, 1 - c, pieces[j]).wait_recv()
         product(1 - c, pieces)
 
     @pl.loop(0, 4)
     def _(i):
         da = offset(i)
-        left, right, far_piece = tid(da, 3), tid(da, 1), tid(da, 2)
+        left, right = tid(da, 3), tid(da, 1)
         b_copy(i, 0, left).wait_recv()
         b_copy(i, 2, left).start()
         d_copy(i, 1, c, left).start()
         b_copy(i, 1, right).wait_recv()
         b_copy(i, 3, right).start()
         d_copy(i, 2, c, right).start()
+        product(c, [tid(da, 0), left, right])
 
         @pl.when(i > 0)
         def _():
-            theirs_in(i - 1)
-
-        b_copy(i, 2, far_piece).wait_recv()
-        b_copy(i, 3, far_piece).wait_recv()
-        d_copy(i, 3, c, far_piece).start()
-        product(c, [tid(da, 0), left, right, far_piece])
-
-        for s in range(3):
-
-            @pl.when(i == s)
-            def _():
-                ring_step(3 + s)
-
-    theirs_in(3)
-    ring_step(6)
+            near_from_partner(i - 1)
+
+    ring_step(3)
+    near_from_partner(3)
+    fars = [tid(da, 2) for da in (0, 3, 1, 2)]
+    for i in range(4):
+        b_copy(i, 2, fars[i]).wait_recv()
+        b_copy(i, 3, fars[i]).wait_recv()
+        d_copy(i, 3, c, fars[i]).start()
+    product(c, fars)
+    ring_step(4)
+    fars = [other_tid(da, 2) for da in (0, 3, 1, 2)]
+    for i in range(4):
+        d_copy(i, 3, 1 - c, fars[i]).wait_recv()
+    product(1 - c, fars)
     exchange(half_state, slices, f_s.at[0], f_r.at[0])
 
     @pl.loop(0, 2 * rows // 80)
@@ -449,6 +456,8 @@
         pown[db] = both[:, 0:LANES]
         pown[db + 1] = both[:, LANES:]
 
+    ring_step(5)
+
     for core in range(2):
         wide_t[core] = wide[core].T
 
@@ -470,13 +479,13 @@
     def _(pair):
         weight_grads(pair)
 
+    ring_step(6)
     exchanged(half_state, slices, f_s.at[0], f_r.at[0])
     running = jnp.zeros((8, 512), F32)
     for e in range(nz):
         scanned[e * 8 : e * 8 + 8, :] = running.astype(BF)
-        running = chip_decay * running + slices[e * 8 : e * 8 + 8, :]
+        running = chip_decay * running + slices[e * 8 : e * 8 + 8, :].astype(F32)
     exchange(scanned, entered.at[rows_here], f_s.at[1], f_r.at[1])
-    ring_step(7)
     for da in (1, 3, 2):
         q_copy(da).wait_recv()
 
@@ -493,6 +502,7 @@
     for da in range(3):
         whole = whole + qbuf[da, 0].astype(F32)
     town[...] = whole
+    ring_step(7)
     for db in (1, 3, 2):
         v_copy(db).wait_recv()
     whole = town[...]
@@ -732,6 +742,14 @@
     def _(k):
         dev = peer(k // 4, lax.rem(k, 4))
         rc(mids.at[c, :, cols], mids.at[c, :, cols], m_s.at[k], m_r.at[k], dev).wait_send()
+
+
+def put_out(*refs):
+    copies = [pltpu.make_async_copy(refs[k], refs[7 + k], refs[14].at[k]) for k in range(7)]
+    for copy in copies:
+        copy.start()
+    for copy in copies:
+        copy.wait()
 
 
 def local(
@@ -795,8 +813,8 @@
             pltpu.VMEM((2, LANES, width), BF),
             pltpu.VMEM((width, 512), BF),
             pltpu.VMEM((2, 256, 512), F32),
-            pltpu.VMEM((128, 512), F32),
-            pltpu.VMEM((128, 512), F32),
+            pltpu.VMEM((128, 512), BF),
+            pltpu.VMEM((128, 512), BF),
             pltpu.VMEM((128, 512), BF),
             pltpu.VMEM((256, 512), F32),
             pltpu.VMEM((2, LANES, 512), BF),
@@ -858,7 +876,7 @@
         name="layer_backward",
     )(
         routes.T,
-        route_weights,
+        route_weights.T,
         cotangent,
         stream,
         gate_proj[0],
@@ -870,6 +888,14 @@
         values,
         decay_rate,
     )
+    grads = pl.pallas_call(
+        put_out,
+        out_shape=shapes,
+        in_specs=[any_] * 7,
+        out_specs=(any_,) * 7,
+        scratch_shapes=[dma((7,))],
+        name="put_out",
+    )(*(pltpu.with_memory_space_constraint(g, pltpu.VMEM) for g in grads))
     return tuple(g[None] for g in grads[:3]) + tuple(grads[3:])
 
 

time: 145 us -> 124 us (0.86)
  Pallas kernels: 137 us -> 122 us
  local copies, waits for them, and re-layouts: 6.36 us -> 0 us
    pallas_call x1, Pallas kernels: 137 us -> 121 us  [local(): pl.pallas_call(functools.partial(kernel, nz), out_shape=tuple((pltpu.VMEM...]
    unnamed x10 -> x0, local copies, waits for them, and re-layouts: 6.36 us -> none
where the time goes in v4:
time: 124 us
  Pallas kernels  122 us (98%)
  between operations  1.45 us (1%)
    pallas_call x1, Pallas kernels, local(): pl.pallas_call(functools.partial(kernel, nz), out_shape=tuple((pltpu.VMEM...  121 us

profile of v4, /device:TPU:1, one launch (start us, length us, event | category | flops | bytes accessed | tf_op | source)
XLA Modules:
  0.0 123.5 jit_solution(16055749614116219042)
XLA Ops:
  1.3 120.7 %layer_backward.1 = (bf16[2048,128]{1,0:T(8,128)(2,1)S(1)}, bf16[2048,128]{1,0:T(8,128)(2,1)S(1)}, bf16[128,2048]{1,0:T(8,128)(2,1)S(1)}, f32[64,512]{1,0:T(8,12...) custom-call(s32[2,128]{1,0:T(2,128)} %bitcast.11, ...), custom_call_target="tpu_custom_call" | custom-call | tf_op jit(solution)/shard_map/layer_backward/pallas_call | solution.py:785
  122.0 1.3 %put_out.1 = (bf16[2048,128]{1,0:T(8,128)(2,1)}, bf16[2048,128]{1,0:T(8,128)(2,1)}, bf16[128,2048]{1,0:T(8,128)(2,1)}, f32[64,512]{1,0:T(8,128)}, bf16[128,256]{...) custom-call(bf16[2048,128]{1,0:T(8,128)(2,1)S(1)} %get-tuple-element.21.refs_0_, ...), custom_call_target="tpu_custom_call" | custom-call | tf_op jit(solution)/shard_map/put_out/pallas_call | solution.py:891
